TPU v7x, 128 devices: a whole 4x4x4 slice. The times are simulated.
128 devices in a mesh: sp: 16 (over z, x), tp: 8 (over y, core).
Axes of the slice: x: 4, y: 4, z: 4, core: 2. Of those that a mesh axis runs over, the one named last changes fastest.
Arguments:
- query_small: bfloat16 [12288, 1024], P('sp', 'tp'), may hold values from -18 to 18
- key_small: bfloat16 [12288, 1024], P('sp', 'tp'), may hold values from -6 to 6
- value_small: bfloat16 [12288, 1024], P('sp', 'tp'), may hold values from -6 to 6
- offset_small: bfloat16 [16, 12288], P('tp', 'sp'), may hold values from -25 to 0
- query_large: bfloat16 [12288, 1024], P('sp', 'tp'), may hold values from -18 to 18
- key_large: bfloat16 [12288, 1024], P('sp', 'tp'), may hold values from -6 to 6
- value_large: bfloat16 [12288, 1024], P('sp', 'tp'), may hold values from -6 to 6
- offset_large: bfloat16 [8, 12288], P('tp', 'sp'), may hold values from -25 to 0
- out_small: bfloat16 [1024, 2048], P('tp'), may hold values from -0.125 to 0.125
- out_large: bfloat16 [1024, 2048], P('tp'), may hold values from -0.125 to 0.125
- residual: bfloat16 [12288, 2048], P(('sp', 'tp')), may hold values from -1.1953125 to 1.1953125
- norm_gain: bfloat16 [2048], replicated, may hold values from 0.099609375 to 1.8984375
- gate_weight: bfloat16 [2048, 5632], P('sp', 'tp'), may hold values from -0.125 to 0.125
- up_weight: bfloat16 [2048, 5632], P('sp', 'tp'), may hold values from -0.125 to 0.125
- down_weight: bfloat16 [5632, 2048], P('tp', 'sp'), may hold values from -0.078125 to 0.078125
Outputs:
- layer_out: bfloat16 [12288, 2048], P(('sp', 'tp'))
All inputs are finite; a program needn't handle non-finite values.
Results may differ from a plain program's by a relative error of at most 0.023.
Values may be sent and summed in bfloat16 or wider, within the bound.
No kernel may reach another device: no remote copies, remote signals or barrier semaphores. Data moves between devices by JAX's collectives and lax.ppermute only.
A program may use at most 128 MiB of HBM per device.

v0:
```python
import jax
import jax.numpy as jnp
import numpy as np
from jax import lax
from jax.experimental import pallas as pl
from jax.experimental.pallas import tpu as pltpu
from jax.sharding import Mesh, PartitionSpec as P


LOG2E = 1.4426950408889634
CEILING = 30.0
BLOCK = 768
RUN = 384
ROWS = 784
LANES = 256
FOLD = 3
SCALES = (64**-0.5 * LOG2E, 64**-0.5 * LOG2E, 128**-0.5 * LOG2E)
SP = ("z", "x")
TP = ("y", "c")


def attention_body(table, q_ref, kv_ref, off_ref, tri_ref, out_ref, totals, *scratch):
    odds, weights, later, total_columns, first_head = scratch
    step = pl.program_id(0)
    kind = table[step]
    key = step % 4
    low = lax.broadcasted_iota(jnp.int32, (RUN, 128), 1) < 64
    zero = jnp.zeros((), jnp.bfloat16)

    def odds_of(slot, head, row, diagonal):
        rows = pl.ds(row, RUN)
        col, queries = (0, slice(0, 128)) if head < 2 else (256, slice(128, 256))
        q = q_ref[0, rows, queries]
        if head == 0:
            q = jnp.where(low, q, zero)
        if head == 1:
            q = jnp.where(low, zero, q)
        for c in range(FOLD):
            keys = kv_ref[key, c * LANES : (c + 1) * LANES, col : col + 128]
            x = lax.dot_general(
                q, keys, (((1,), (1,)), ((), ())), preferred_element_type=jnp.float32
            )
            x = x * SCALES[head] + off_ref[key, head, c : c + 1, :]
            e = jnp.exp2(jnp.minimum(x, CEILING))
            if diagonal:
                t = lax.broadcasted_iota(jnp.int32, (RUN, LANES), 0) + row
                s = lax.broadcasted_iota(jnp.int32, (RUN, LANES), 1) * FOLD + c
                e = jnp.where(s < t, e, 0.0)
            odds[slot, c] = e

    def suffix_of(slot, head, row):
        rows = pl.ds(row, RUN)
        log_pass = jnp.log2((1.0 + odds[slot, 0]) * (1.0 + odds[slot, 1]) * (1.0 + odds[slot, 2]))
        short = (-log_pass).astype(jnp.bfloat16)
        after = jnp.dot(short, tri_ref[...], preferred_element_type=jnp.float32)
        later[slot] = after - log_pass
        total = after[:, :1] + short[:, :1].astype(jnp.float32)
        lane = lax.broadcasted_iota(jnp.int32, (RUN, 128), 1)
        total_columns[rows] = jnp.where(lane == step * 3 + head, total, total_columns[rows])

    def mixed_of(slot, head, row):
        rows = pl.ds(row, RUN)
        scale = jnp.exp2(later[slot])
        for c in range(FOLD):
            e = odds[slot, c]
            weights[slot, :, c * LANES : (c + 1) * LANES] = (e * scale).astype(jnp.bfloat16)
            if c + 1 < FOLD:
                scale = scale * (1.0 + e)
        col = 128 if head < 2 else 384
        values = kv_ref[key, :BLOCK, col : col + 128]
        result = jnp.dot(weights[slot], values, preferred_element_type=jnp.float32)
        if head == 0:
            first_head[rows] = result
        elif head == 1:
            out_ref[0, rows, :128] = jnp.where(low, first_head[rows], result).astype(jnp.bfloat16)
        else:
            out_ref[0, rows, 128:] = result.astype(jnp.bfloat16)

    def sweep(runs, diagonal):
        for t in range(len(runs) + 2):
            if t < len(runs):
                odds_of(t % 3, *runs[t], diagonal)
            if 0 <= t - 1 < len(runs):
                suffix_of((t - 1) % 3, *runs[t - 1])
            if 0 <= t - 2:
                mixed_of((t - 2) % 3, *runs[t - 2])

    @pl.when(step == 0)
    def _():
        total_columns[...] = jnp.zeros_like(total_columns)

    @pl.when(kind == 0)
    def _():
        out_ref[...] = jnp.zeros_like(out_ref)

    @pl.when(kind == 1)
    def _():
        sweep([(head, row) for head in range(3) for row in range(0, BLOCK, RUN)], False)

    @pl.when(kind == 2)
    def _():
        def one(i, _):
            sweep([(head, pl.multiple_of(i * RUN, RUN)) for head in range(3)], True)
            return 0

        lax.fori_loop(0, BLOCK // RUN, one, 0)

    @pl.when(step == 15)
    def _():
        totals[...] = jnp.transpose(total_columns[...])[:48]


def attention(kinds, queries, kv, offsets):
    tri = jnp.asarray(np.tril(np.ones((LANES, LANES)), -1), jnp.bfloat16)
    return pl.pallas_call(
        attention_body,
        grid_spec=pltpu.PrefetchScalarGridSpec(
            num_scalar_prefetch=1,
            grid=(16,),
            in_specs=[
                pl.BlockSpec((1, BLOCK, 256), lambda i, t: (i // 4, 0, 0)),
                pl.BlockSpec((4, ROWS, 512), lambda i, t: (0, 0, 0)),
                pl.BlockSpec((4, 3, 4, LANES), lambda i, t: (0, 0, 0, 0)),
                pl.BlockSpec((LANES, LANES), lambda i, t: (0, 0)),
            ],
            out_specs=[
                pl.BlockSpec((1, BLOCK, 256), lambda i, t: (i, 0, 0)),
                pl.BlockSpec((48, BLOCK), lambda i, t: (0, 0)),
            ],
            scratch_shapes=[
                pltpu.VMEM((3, FOLD, RUN, LANES), jnp.float32),
                pltpu.VMEM((3, RUN, BLOCK), jnp.bfloat16),
                pltpu.VMEM((3, RUN, LANES), jnp.float32),
                pltpu.VMEM((BLOCK, 128), jnp.float32),
                pltpu.VMEM((BLOCK, 128), jnp.float32),
            ],
        ),
        out_shape=[
            jax.ShapeDtypeStruct((16, BLOCK, 256), jnp.bfloat16),
            jax.ShapeDtypeStruct((48, BLOCK), jnp.float32),
        ],
        compiler_params=pltpu.CompilerParams(
            dimension_semantics=("arbitrary",), vmem_limit_bytes=40 * 2**20
        ),
        name="stick_attention",
    )(kinds, queries, kv, offsets, tri)


def combine_body(place, outs, t0, t1, t2, t3, part, factors):
    i = pl.program_id(0)
    z, x = place[0], place[1]
    tables = (t0, t1, t2, t3)
    factors[...] = jnp.zeros_like(factors)

    def flag(condition):
        return jnp.where(condition, 1.0, 0.0)

    for head in range(3):
        whole, above = [], []
        for j in range(4):
            rows = [
                tables[k][pl.ds(((i - k + 4) % 4 * 4 + j) * 3 + head, 1), :] for k in range(4)
            ]
            whole.append(rows[0] + rows[1] + rows[2] + rows[3])
            above.append(sum(rows[k] * flag((x + k) % 4 > x) for k in range(1, 4)))
        for j in range(4):
            later = above[j]
            for other in range(4):
                if other != j:
                    later = later + whole[other] * flag((z + other) % 4 > (z + j) % 4)
            factors[j * 3 + head : j * 3 + head + 1, :] = jnp.exp2(later)
    turned = jnp.transpose(factors[...])
    low = lax.broadcasted_iota(jnp.int32, (BLOCK, 128), 1) < 64
    small = large = 0.0
    for j in range(4):
        f = [turned[:, 3 * j + head : 3 * j + head + 1] for head in range(3)]
        small = small + outs[j, :, :128].astype(jnp.float32) * jnp.where(low, f[0], f[1])
        large = large + outs[j, :, 128:].astype(jnp.float32) * f[2]
    part[0, :, :128] = small.astype(jnp.bfloat16)
    part[0, :, 128:] = large.astype(jnp.bfloat16)


def combine(place, outs, tables):
    whole = pl.BlockSpec((48, BLOCK), lambda i, p: (0, 0))
    return pl.pallas_call(
        combine_body,
        grid_spec=pltpu.PrefetchScalarGridSpec(
            num_scalar_prefetch=1,
            grid=(4,),
            in_specs=[pl.BlockSpec((4, BLOCK, 256), lambda i, p: (i, 0, 0))] + [whole] * 4,
            out_specs=pl.BlockSpec((1, BLOCK, 256), lambda i, p: (i, 0, 0)),
            scratch_shapes=[pltpu.VMEM((128, BLOCK), jnp.float32)],
        ),
        out_shape=jax.ShapeDtypeStruct((4, BLOCK, 256), jnp.bfloat16),
        compiler_params=pltpu.CompilerParams(
            dimension_semantics=("arbitrary",), vmem_limit_bytes=24 * 2**20
        ),
        name="combine_key_blocks",
    )(place, outs, *tables)


def balanced(back):
    pairs = []
    for z in range(4):
        for x in range(4):
            chunk = 2 * z + x // 2
            to = 4 * (chunk if chunk < 4 else 7 - chunk) + x
            pairs.append((to, 4 * z + x) if back else (4 * z + x, to))
    return pairs


def tile_kinds(z, x):
    home = np.zeros(16, np.int32)
    for source, to in balanced(False):
        home[to] = source
    ahead = jnp.arange(4, dtype=jnp.int32)
    query = jnp.asarray(home)[4 * z + (x + ahead) % 4]
    key = 4 * ((z + ahead) % 4) + x
    before = (key[None, :] < query[:, None]).astype(jnp.int32)
    same = (key[None, :] == query[:, None]).astype(jnp.int32)
    return (before + 2 * same).reshape(16)


def packed_keys(key_small, value_small, offset_small, key_large, value_large, offset_large):
    rows = jnp.concatenate([key_small, value_small, key_large, value_large], axis=1)
    rows = rows.reshape(LANES, FOLD, 512).transpose(1, 0, 2).reshape(BLOCK, 512)
    offsets = jnp.concatenate([offset_small, offset_large], axis=0)
    offsets = offsets.reshape(3, LANES, FOLD).transpose(0, 2, 1).reshape(3, BLOCK)
    offsets = jnp.pad(offsets, ((0, 0), (0, 1024 - BLOCK))).reshape(6, 512)
    offsets = jnp.pad(offsets, ((0, ROWS - BLOCK - 6), (0, 0)))
    return jnp.concatenate([rows, offsets], axis=0)


def mlp_body(place, *refs):
    (ma, mb, na, nb, r_own, r_other, gain, o_own, o_other, w_hbm) = refs[:10]
    own_out, mine_out, theirs_out = refs[10:13]
    rows, normed, out_w, w, sems = refs[13:]
    step = pl.program_id(0)
    core = place[1]
    copies = [
        pltpu.make_async_copy(o_own, out_w.at[0:1024], sems.at[0]),
        pltpu.make_async_copy(o_other, out_w.at[1024:2048], sems.at[1]),
        pltpu.make_async_copy(w_hbm, w, sems.at[2]),
    ]

    @pl.when(step == 0)
    def _():
        for copy in copies:
            copy.start()

    rows[:192, :1024] = ma[0]
    rows[192:, :1024] = mb[0]
    rows[:192, 1024:] = na[0]
    rows[192:, 1024:] = nb[0]

    @pl.when(step == 0)
    def _():
        copies[0].wait()
        copies[1].wait()

    part = jnp.dot(rows[...], out_w[...], preferred_element_type=jnp.float32)
    attended = part.astype(jnp.bfloat16).astype(jnp.float32)
    kept = []
    for k in range(2):
        mine, theirs = r_own[k].astype(jnp.float32), r_other[k].astype(jnp.float32)
        kept += [jnp.where(core == 0, mine, theirs), jnp.where(core == 0, theirs, mine)]
    kept = jnp.concatenate(kept, axis=0)
    stream = kept + attended
    scale = lax.rsqrt(jnp.mean(stream * stream, axis=-1, keepdims=True) + 1e-06)
    normed[...] = (stream * scale * gain[...].astype(jnp.float32)).astype(jnp.bfloat16)

    @pl.when(step == 0)
    def _():
        own_out[...] = jnp.where(core == 0, stream[0:96], stream[96:192])
        copies[2].wait()

    both = jnp.dot(normed[...], w[:, :1408], preferred_element_type=jnp.float32)
    gate, upper = both[:, :704], both[:, 704:]
    hidden = (gate / (1.0 + jnp.exp(-gate)) * upper).astype(jnp.bfloat16)
    down = lax.dot_general(
        hidden, w[:, 1408:], (((1,), (1,)), ((), ())), preferred_element_type=jnp.float32
    )
    for k in range(2):
        one, two = down[192 * k : 192 * k + 96], down[192 * k + 96 : 192 * k + 192]
        mine_out[k] = jnp.where(core == 0, one, two).astype(jnp.bfloat16)
        theirs_out[k] = jnp.where(core == 0, two, one).astype(jnp.bfloat16)


def mlp(place, m_own, m_other, r_own, r_other, gain, o_own, o_other, w):
    def at(k):
        return lambda g, p: ((p[0] + 2 * g + k) % 4, 0, 0)

    m_own, m_other = m_own.reshape(4, 192, 1024), m_other.reshape(4, 192, 1024)
    return pl.pallas_call(
        mlp_body,
        grid_spec=pltpu.PrefetchScalarGridSpec(
            num_scalar_prefetch=1,
            grid=(2,),
            in_specs=[
                pl.BlockSpec((1, 192, 1024), at(0)),
                pl.BlockSpec((1, 192, 1024), at(1)),
                pl.BlockSpec((1, 192, 1024), at(0)),
                pl.BlockSpec((1, 192, 1024), at(1)),
                pl.BlockSpec((2, 96, 2048), lambda g, p: (g, 0, 0)),
                pl.BlockSpec((2, 96, 2048), lambda g, p: (g, 0, 0)),
                pl.BlockSpec((1, 2048), lambda g, p: (0, 0)),
                pl.BlockSpec(memory_space=pl.ANY),
                pl.BlockSpec(memory_space=pl.ANY),
                pl.BlockSpec(memory_space=pl.ANY),
            ],
            out_specs=[
                pl.BlockSpec((96, 2048), lambda g, p: (0, 0)),
                pl.BlockSpec((2, 96, 2048), lambda g, p: (g, 0, 0)),
                pl.BlockSpec((2, 96, 2048), lambda g, p: (g, 0, 0)),
            ],
            scratch_shapes=[
                pltpu.VMEM((384, 2048), jnp.bfloat16),
                pltpu.VMEM((384, 2048), jnp.bfloat16),
                pltpu.VMEM((2048, 2048), jnp.bfloat16),
                pltpu.VMEM((2048, 2112), jnp.bfloat16),
                pltpu.SemaphoreType.DMA((3,)),
            ],
        ),
        out_shape=[
            jax.ShapeDtypeStruct((96, 2048), jnp.float32),
            jax.ShapeDtypeStruct((4, 96, 2048), jnp.bfloat16),
            jax.ShapeDtypeStruct((4, 96, 2048), jnp.bfloat16),
        ],
        compiler_params=pltpu.CompilerParams(
            dimension_semantics=("arbitrary",), vmem_limit_bytes=58 * 2**20
        ),
        name="project_norm_mlp",
    )(place, m_own, m_own, m_other, m_other, r_own, r_other, gain, o_own, o_other, w)


def ring(k):
    return [(i, (i + k) % 4) for i in range(4)]


def swapped(a):
    return lax.ppermute(a, "c", [(0, 1), (1, 0)])


def ring_gather(a, axis, dim):
    h = a.shape[0] // 2
    before = lax.ppermute(a, axis, ring(1))
    after = lax.ppermute(a, axis, ring(3))
    top = lax.ppermute(before[:h], axis, ring(1))
    bottom = lax.ppermute(after[h:], axis, ring(3))
    opposite = jnp.concatenate([top, bottom], axis=0)
    if dim is None:
        return jnp.stack([a, after, opposite, before])
    return jnp.concatenate([a, after, opposite, before], axis=dim)


def passed_on(before, after, axis):
    h = before.shape[0] // 2
    top = lax.ppermute(before[:h], axis, ring(1))
    bottom = lax.ppermute(after[h:], axis, ring(3))
    return top, bottom


def together(a, before, after, opposite):
    return jnp.stack([a, after, jnp.concatenate(opposite, axis=0), before])


def exchanged(pieces, axis):
    h = pieces.shape[1] // 2
    after = lax.ppermute(pieces[1], axis, ring(1))
    before = lax.ppermute(pieces[3], axis, ring(3))
    top = lax.ppermute(pieces[2, :h], axis, ring(2))
    bottom = lax.ppermute(pieces[2, h:], axis, ring(-2))
    opposite = jnp.concatenate([top, bottom], axis=0).astype(jnp.float32)
    near = pieces[0].astype(jnp.float32) + after.astype(jnp.float32) + before.astype(jnp.float32)
    return near + opposite


def on_device(
    query_small,
    key_small,
    value_small,
    offset_small,
    query_large,
    key_large,
    value_large,
    offset_large,
    out_small,
    out_large,
    residual,
    norm_gain,
    gate_weight,
    up_weight,
    down_weight,
):
    z, x = lax.axis_index("z"), lax.axis_index("x")
    y, core = lax.axis_index("y"), lax.axis_index("c")
    kinds = tile_kinds(z, x)
    queries = jnp.concatenate([query_small, query_large], axis=1)
    kv = packed_keys(key_small, value_small, offset_small, key_large, value_large, offset_large)
    kv, queries = lax.optimization_barrier((kv, queries))
    kv_before = lax.ppermute(kv, "z", ring(1))
    kv_after = lax.ppermute(kv, "z", ring(3))
    queries = lax.ppermute(queries, SP, balanced(False))
    q_before = lax.ppermute(queries, "x", ring(1))
    q_after = lax.ppermute(queries, "x", ring(3))
    w = jnp.concatenate([gate_weight, up_weight, down_weight.T], axis=1)
    q_after, w = lax.optimization_barrier((q_after, w))
    w = lax.all_gather(w, SP, axis=0, tiled=True)
    kv = together(kv, kv_before, kv_after, passed_on(kv_before, kv_after, "z"))
    queries = together(queries, q_before, q_after, passed_on(q_before, q_after, "x"))
    outs_in = jnp.concatenate([out_small, out_large], axis=0)
    o_before = lax.ppermute(outs_in, "y", ring(1))
    o_after = lax.ppermute(outs_in, "y", ring(3))
    offsets = kv[:, BLOCK : BLOCK + 6].reshape(4, 3, 4, LANES).astype(jnp.float32) * LOG2E

    kv, queries, offsets, kinds, o_before, o_after, residual = lax.optimization_barrier(
        (kv, queries, offsets, kinds, o_before, o_after, residual)
    )
    r_before = lax.ppermute(residual, "y", ring(1))
    r_after = lax.ppermute(residual, "y", ring(3))
    o_opposite = passed_on(o_before, o_after, "y")
    outs, totals = attention(kinds, queries, kv, offsets)
    outs, totals, r_before, r_after, o_opposite = lax.optimization_barrier(
        (outs, totals, r_before, r_after, o_opposite)
    )
    o_own = together(outs_in, o_before, o_after, o_opposite).reshape(1024, 2048)
    from_before = lax.ppermute(totals, "x", ring(1))
    from_after = lax.ppermute(totals, "x", ring(3))
    from_opposite = lax.ppermute(totals, "x", ring(2))
    spot = jnp.stack([z, x]).astype(jnp.int32)
    o_other = swapped(o_own)
    r_opposite = passed_on(r_before, r_after, "y")
    r_own = together(residual, r_before, r_after, r_opposite)
    r_other = swapped(r_own)
    part = combine(spot, outs, (totals, from_after, from_opposite, from_before))
    mixed = exchanged(part, "x").astype(jnp.bfloat16)
    mixed = lax.ppermute(mixed, SP, balanced(True))
    m_own = ring_gather(mixed, "y", 1)
    m_other = swapped(m_own)
    place = jnp.stack([y, core]).astype(jnp.int32)
    stream, mine, theirs = mlp(
        place, m_own, m_other, r_own, r_other, norm_gain.reshape(1, -1), o_own, o_other, w
    )
    f32 = jnp.float32
    pair = (mine.astype(f32) + swapped(theirs).astype(f32)).astype(jnp.bfloat16)
    summed = exchanged(pair, "y")
    return (stream + summed.astype(jnp.bfloat16).astype(f32)).astype(jnp.bfloat16)


def solution(mesh):
    named = Mesh(mesh.devices.reshape(4, 4, 4, 2), SP + TP)

    return jax.shard_map(
        on_device,
        mesh=named,
        in_specs=(
            P(SP, TP),
            P(SP, TP),
            P(SP, TP),
            P(TP, SP),
            P(SP, TP),
            P(SP, TP),
            P(SP, TP),
            P(TP, SP),
            P(TP, None),
            P(TP, None),
            P(SP + TP, None),
            P(),
            P(SP, TP),
            P(SP, TP),
            P(TP, SP),
        ),
        out_specs=P(SP + TP, None),
        check_vma=False,
    )
```

profile of v0, /device:TPU:96, one launch (start us, length us, event | category | flops | bytes accessed | tf_op | source)
XLA Modules:
  0.0 262.8 jit_solution(13558009131763822996)
XLA Ops:
  12.8 10.3 %collective-permute-done.4 = bf16[768,256]{1,0:T(8,128)(2,1)S(1)} collective-permute-done((bf16[768,256]{1,0:T(8,128)(2,1)S(1)}, bf16[768,256]{1,0:T(8,128)(2,1)S(1)}, u32[]{:S(2)}, u32[]{:S(2)}) %collective-permute-start.4) | collective-permute-done | bytes 393248 | tf_op jit(solution)/shard_map/ppermute | solution.py:403
  23.1 4.3 %collective-permute-start.5 = (bf16[768,256]{1,0:T(8,128)(2,1)S(1)}, bf16[768,256]{1,0:T(8,128)(2,1)S(1)}, u32[]{:S(2)}, u32[]{:S(2)}) collective-permute-start(bf16[768,256]{1,0:T(8,128)(2,1)S(1)} %collective-permute-done.4), channel_id=1, source_target_pairs={{0,24},{8,0},{16,8},{24,16},{1,25},{9,1},{17,9},{25,17},{2,26},{10... | collective-permute-start | bytes 1179656 | tf_op jit(solution)/shard_map/ppermute | solution.py:405
  28.9 6.0 %collective-permute-done.5 = bf16[768,256]{1,0:T(8,128)(2,1)S(1)} collective-permute-done((bf16[768,256]{1,0:T(8,128)(2,1)S(1)}, bf16[768,256]{1,0:T(8,128)(2,1)S(1)}, u32[]{:S(2)}, u32[]{:S(2)}) %collective-permute-start.5) | collective-permute-done | bytes 393248 | tf_op jit(solution)/shard_map/ppermute | solution.py:405
  49.2 9.9 %collective-permute-done.1 = bf16[784,512]{1,0:T(8,128)(2,1)S(1)} collective-permute-done((bf16[784,512]{1,0:T(8,128)(2,1)S(1)}, bf16[784,512]{1,0:T(8,128)(2,1)S(1)}, u32[]{:S(2)}, u32[]{:S(2)}) %collective-permute-start.1) | collective-permute-done | bytes 802848 | tf_op jit(solution)/shard_map/ppermute | solution.py:401
  59.0 5.7 %collective-permute-start.8 = (bf16[384,256]{1,0:T(8,128)(2,1)S(1)}, bf16[384,256]{1,0:T(8,128)(2,1)}, u32[]{:S(2)}, u32[]{:S(2)}) collective-permute-start(bf16[384,256]{1,0:T(8,128)(2,1)S(1)} %slice.66), channel_id=1, source_target_pairs={{0,24},{8,0},{16,8},{24,16},{1,25},{9,1},{17,9},{25,17},{2,26},{10... | collective-permute-start | bytes 589832 | tf_op jit(solution)/shard_map/ppermute | solution.py:359
  73.6 4.5 %collective-permute-done.3 = bf16[392,512]{1,0:T(8,128)(2,1)} collective-permute-done((bf16[392,512]{1,0:T(8,128)(2,1)}, bf16[392,512]{1,0:T(8,128)(2,1)}, u32[]{:S(2)}, u32[]{:S(2)}) %collective-permute-start.3) | collective-permute-done | bytes 401440 | tf_op jit(solution)/shard_map/ppermute | solution.py:359
  83.1 4.1 %collective-permute-start.14 = (bf16[128,2048]{1,0:T(8,128)(2,1)S(1)}, bf16[128,2048]{1,0:T(8,128)(2,1)S(1)}, u32[]{:S(2)}, u32[]{:S(2)}) collective-permute-start(bf16[128,2048]{1,0:T(8,128)(2,1)S(1)} %slice.69), channel_id=1, source_target_pairs={{0,6},{2,0},{4,2},{6,4},{1,7},{3,1},{5,3},{7,5},{8,14},{10,8},{12,... | collective-permute-start | bytes 1572872 | tf_op jit(solution)/shard_map/ppermute | solution.py:359
  87.2 3.2 %collective-permute-start.12 = (bf16[96,2048]{1,0:T(8,128)(2,1)S(1)}, bf16[96,2048]{1,0:T(8,128)(2,1)S(1)}, u32[]{:S(2)}, u32[]{:S(2)}) collective-permute-start(bf16[96,2048]{1,0:T(8,128)(2,1)S(1)} %copy-done.11), channel_id=1, source_target_pairs={{0,6},{2,0},{4,2},{6,4},{1,7},{3,1},{5,3},{7,5},{8,14},{10,8},{12,... | collective-permute-start | bytes 1179656 | tf_op jit(solution)/shard_map/ppermute | solution.py:420
  90.4 34.5 %stick_attention.1 = (bf16[16,768,256]{2,1,0:T(8,128)(2,1)S(1)}, f32[48,768]{1,0:T(8,128)S(1)}) custom-call(s32[16]{0:T(128)S(1)} %add.124.table, bf16[4,768,256]{2,1,0:T(8,128)(2,1)S(1)} %copy-done, bf16[4,784,512]{2,1,0:T(8,128)(2,1)S(1)} %pad_maximum_fusion.1.kv_ref, f32[4,3,4,256]{3,2,1,0:T(4,128)S(1)} %mul.24.off_ref, bf16[256,256]{1,0:T(8,128)(2,1)S(1)} %copy-done.1), custom_call_target="tpu_custom_call" | custom-call | tf_op jit(solution)/shard_map/stick_attention/pallas_call | solution.py:115
  125.1 3.7 %pad_maximum_fusion = bf16[4,256,2048]{2,1,0:T(8,128)(2,1)} fusion(bf16[1,256,2048]{2,1,0:T(8,128)(2,1)} %bitcast.31, bf16[1,256,2048]{2,1,0:T(8,128)(2,1)S(1)} %maximum_bitcast_fusion, bf16[1,256,2048]{2,1,0:T(8,128)(2,1)} %bitcast.29, bf16[1,256,2048]{2,1,0:T(8,128)(2,1)} %bitcast.28), kind=kLoop, calls=%fused_computation.1 | loop fusion | flops 6291456 | bytes 8388608 | tf_op jit(solution)/shard_map/stack | solution.py:364
  132.1 7.3 %collective-permute-done.17.t3 = f32[48,768]{1,0:T(8,128)S(1)} collective-permute-done((f32[48,768]{1,0:T(8,128)S(1)}, f32[48,768]{1,0:T(8,128)S(1)}, u32[]{:S(2)}, u32[]{:S(2)}) %collective-permute-start.17) | collective-permute-done | bytes 147488 | tf_op jit(solution)/shard_map/ppermute | solution.py:427
  140.0 7.3 %combine_key_blocks.1 = bf16[4,768,256]{2,1,0:T(8,128)(2,1)S(1)} custom-call(s32[2]{0:T(128)S(1)} %pad_add_fusion.1.place, bf16[16,768,256]{2,1,0:T(8,128)(2,1)S(1)} %get-tuple-element.39.outs, f32[48,768]{1,0:T(8,128)S(1)} %get-tuple-element.40.t0, f32[48,768]{1,0:T(8,128)S(1)} %collective-permute-done.15.t1, f32[48,768]{1,0:T(8,128)S(1)} %collective-permute-done.16.t2, ...), custom_call_target="tpu_custom_call" | custom-call | tf_op jit(solution)/shard_map/combine_key_blocks/pallas_call | solution.py:185
  154.3 11.1 %collective-permute-done.20 = bf16[384,256]{1,0:T(8,128)(2,1)S(1)} collective-permute-done((bf16[384,256]{1,0:T(8,128)(2,1)S(1)}, bf16[384,256]{1,0:T(8,128)(2,1)S(1)}, u32[]{:S(2)}, u32[]{:S(2)}) %collective-permute-start.20) | collective-permute-done | bytes 196640 | tf_op jit(solution)/shard_map/ppermute | solution.py:371
  170.7 3.3 %collective-permute-start.29 = (bf16[48,2048]{1,0:T(8,128)(2,1)S(1)}, bf16[48,2048]{1,0:T(8,128)(2,1)S(1)}, u32[]{:S(2)}, u32[]{:S(2)}) collective-permute-start(bf16[48,2048]{1,0:T(8,128)(2,1)S(1)} %slice.78), channel_id=1, source_target_pairs={{0,6},{2,0},{4,2},{6,4},{1,7},{3,1},{5,3},{7,5},{8,14},{10,8},{12,... | collective-permute-start | bytes 589832 | tf_op jit(solution)/shard_map/ppermute | solution.py:359
  173.9 7.9 %collective-permute-done.22 = bf16[768,256]{1,0:T(8,128)(2,1)S(1)} collective-permute-done((bf16[768,256]{1,0:T(8,128)(2,1)S(1)}, bf16[768,256]{1,0:T(8,128)(2,1)S(1)}, u32[]{:S(2)}, u32[]{:S(2)}) %collective-permute-start.22) | collective-permute-done | bytes 393248 | tf_op jit(solution)/shard_map/ppermute | solution.py:437
  181.9 3.2 %collective-permute-start.23 = (bf16[768,256]{1,0:T(8,128)(2,1)S(1)}, bf16[768,256]{1,0:T(8,128)(2,1)S(1)}, u32[]{:S(2)}, u32[]{:S(2)}) collective-permute-start(bf16[768,256]{1,0:T(8,128)(2,1)S(1)} %collective-permute-done.22), channel_id=1, source_target_pairs={{0,6},{2,0},{4,2},{6,4},{1,7},{3,1},{5,3},{7,5},{8,14},{10,8},{12,... | collective-permute-start | bytes 1179656 | tf_op jit(solution)/shard_map/ppermute | solution.py:347
  185.2 7.2 %collective-permute-done.24 = bf16[768,256]{1,0:T(8,128)(2,1)S(1)} collective-permute-done((bf16[768,256]{1,0:T(8,128)(2,1)S(1)}, bf16[768,256]{1,0:T(8,128)(2,1)S(1)}, u32[]{:S(2)}, u32[]{:S(2)}) %collective-permute-start.24) | collective-permute-done | bytes 393248 | tf_op jit(solution)/shard_map/ppermute | solution.py:346
  192.8 3.3 %collective-permute-start.26 = (bf16[384,256]{1,0:T(8,128)(2,1)S(1)}, bf16[384,256]{1,0:T(8,128)(2,1)S(1)}, u32[]{:S(2)}, u32[]{:S(2)}) collective-permute-start(bf16[384,256]{1,0:T(8,128)(2,1)S(1)} %slice.96), channel_id=1, source_target_pairs={{0,6},{2,0},{4,2},{6,4},{1,7},{3,1},{5,3},{7,5},{8,14},{10,8},{12,... | collective-permute-start | bytes 589832 | tf_op jit(solution)/shard_map/ppermute | solution.py:349
  196.4 3.2 %collective-permute-done.25 = bf16[384,256]{1,0:T(8,128)(2,1)S(1)} collective-permute-done((bf16[384,256]{1,0:T(8,128)(2,1)S(1)}, bf16[384,256]{1,0:T(8,128)(2,1)S(1)}, u32[]{:S(2)}, u32[]{:S(2)}) %collective-permute-start.25) | collective-permute-done | bytes 196640 | tf_op jit(solution)/shard_map/ppermute | solution.py:348
  203.5 23.3 %project_norm_mlp.1 = (f32[96,2048]{1,0:T(8,128)}, bf16[4,96,2048]{2,1,0:T(8,128)(2,1)}, bf16[4,96,2048]{2,1,0:T(8,128)(2,1)}) custom-call(s32[2]{0:T(128)} %pad_add_fusion.place, bf16[4,192,1024]{2,1,0:T(8,128)(2,1)} %bitcast.61, bf16[4,192,1024]{2,1,0:T(8,128)(2,1)} %bitcast.62, bf16[4,192,1024]{2,1,0:T(8,128)(2,1)} %bitcast.23.refs_2_.refs_3_, ...), custom_call_target="tpu_custom_call" | custom-call | tf_op jit(solution)/shard_map/project_norm_mlp/pallas_call | solution.py:294
  227.0 3.5 %collective-permute-done.32 = bf16[4,96,2048]{2,1,0:T(8,128)(2,1)S(1)} collective-permute-done((bf16[4,96,2048]{2,1,0:T(8,128)(2,1)}, bf16[4,96,2048]{2,1,0:T(8,128)(2,1)S(1)}, u32[]{:S(2)}, u32[]{:S(2)}) %collective-permute-start.32) | collective-permute-done | bytes 1572896 | tf_op jit(solution)/shard_map/ppermute | solution.py:341
  232.7 3.4 %collective-permute-start.34 = (bf16[96,2048]{1,0:T(8,128)(2,1)S(1)}, bf16[96,2048]{1,0:T(8,128)(2,1)S(1)}, u32[]{:S(2)}, u32[]{:S(2)}) collective-permute-start(bf16[96,2048]{1,0:T(8,128)(2,1)S(1)} %get-tuple-element.52), channel_id=1, source_target_pairs={{0,6},{2,0},{4,2},{6,4},{1,7},{3,1},{5,3},{7,5},{8,14},{10,8},{12,... | collective-permute-start | bytes 1179656 | tf_op jit(solution)/shard_map/ppermute | solution.py:370
  239.7 11.9 %collective-permute-done.35 = bf16[48,2048]{1,0:T(8,128)(2,1)S(1)} collective-permute-done((bf16[48,2048]{1,0:T(8,128)(2,1)S(1)}, bf16[48,2048]{1,0:T(8,128)(2,1)S(1)}, u32[]{:S(2)}, u32[]{:S(2)}) %collective-permute-start.35) | collective-permute-done | bytes 196640 | tf_op jit(solution)/shard_map/ppermute | solution.py:371
  251.6 3.4 %collective-permute-done.36 = bf16[48,2048]{1,0:T(8,128)(2,1)S(1)} collective-permute-done((bf16[48,2048]{1,0:T(8,128)(2,1)S(1)}, bf16[48,2048]{1,0:T(8,128)(2,1)S(1)}, u32[]{:S(2)}, u32[]{:S(2)}) %collective-permute-start.36) | collective-permute-done | bytes 196640 | tf_op jit(solution)/shard_map/ppermute | solution.py:372
  (148 shorter events, 63.4 us)
Async XLA Ops:
  6.5 196.9 %all-gather.2.cloned.1.call-start = ((), (), s32[]{:S(2)}) async-start(), calls=%async_computation | async-start | bytes 9469952 | tf_op jit(solution)/shard_map/all_gather | solution.py:408
  10.2 12.9 %collective-permute-start.4 = (bf16[768,256]{1,0:T(8,128)(2,1)S(1)}, bf16[768,256]{1,0:T(8,128)(2,1)S(1)}, u32[]{:S(2)}, u32[]{:S(2)}) collective-permute-start(bf16[768,256]{1,0:T(8,128)(2,1)S(1)} %pad_maximum_fusion.6), channel_id=1, source_target_pairs={{0,0},{8,8},{16,48},{24,56},{32,64},{40,72},{48,112},{56,120},{64,... | collective-permute-start | bytes 1179656 | tf_op jit(solution)/shard_map/ppermute | solution.py:403
  23.1 11.8 %collective-permute-start.5 = (bf16[768,256]{1,0:T(8,128)(2,1)S(1)}, bf16[768,256]{1,0:T(8,128)(2,1)S(1)}, u32[]{:S(2)}, u32[]{:S(2)}) collective-permute-start(bf16[768,256]{1,0:T(8,128)(2,1)S(1)} %collective-permute-done.4), channel_id=1, source_target_pairs={{0,24},{8,0},{16,8},{24,16},{1,25},{9,1},{17,9},{25,17},{2,26},{10... | collective-permute-start | bytes 1179656 | tf_op jit(solution)/shard_map/ppermute | solution.py:405
  34.9 24.1 %collective-permute-start.1 = (bf16[784,512]{1,0:T(8,128)(2,1)S(1)}, bf16[784,512]{1,0:T(8,128)(2,1)S(1)}, u32[]{:S(2)}, u32[]{:S(2)}) collective-permute-start(bf16[784,512]{1,0:T(8,128)(2,1)S(1)} %fusion.1), channel_id=1, source_target_pairs={{0,32},{32,64},{64,96},{96,0},{1,33},{33,65},{65,97},{97,1},{2,34}... | collective-permute-start | bytes 2408456 | tf_op jit(solution)/shard_map/ppermute | solution.py:401
  35.3 30.3 %collective-permute-start = (bf16[784,512]{1,0:T(8,128)(2,1)S(1)}, bf16[784,512]{1,0:T(8,128)(2,1)S(1)}, u32[]{:S(2)}, u32[]{:S(2)}) collective-permute-start(bf16[784,512]{1,0:T(8,128)(2,1)S(1)} %fusion.1), channel_id=1, source_target_pairs={{0,96},{32,0},{64,32},{96,64},{1,97},{33,1},{65,33},{97,65},{2,98}... | collective-permute-start | bytes 2408456 | tf_op jit(solution)/shard_map/ppermute | solution.py:402
  41.8 39.0 %collective-permute-start.10 = (bf16[256,2048]{1,0:T(8,128)(2,1)}, bf16[256,2048]{1,0:T(8,128)(2,1)}, u32[]{:S(2)}, u32[]{:S(2)}) collective-permute-start(bf16[256,2048]{1,0:T(8,128)(2,1)} %constant_dynamic-update-slice_fusion), channel_id=1, source_target_pairs={{0,6},{2,0},{4,2},{6,4},{1,7},{3,1},{5,3},{7,5},{8,14},{10,8},{12,... | collective-permute-start | bytes 3145736 | tf_op jit(solution)/shard_map/ppermute | solution.py:413
  44.8 35.9 %collective-permute-start.9 = (bf16[256,2048]{1,0:T(8,128)(2,1)}, bf16[256,2048]{1,0:T(8,128)(2,1)}, u32[]{:S(2)}, u32[]{:S(2)}) collective-permute-start(bf16[256,2048]{1,0:T(8,128)(2,1)} %constant_dynamic-update-slice_fusion), channel_id=1, source_target_pairs={{0,2},{2,4},{4,6},{6,0},{1,3},{3,5},{5,7},{7,1},{8,10},{10,12},{12... | collective-permute-start | bytes 3145736 | tf_op jit(solution)/shard_map/ppermute | solution.py:412
  48.5 18.4 %collective-permute-start.7 = (bf16[384,256]{1,0:T(8,128)(2,1)}, bf16[384,256]{1,0:T(8,128)(2,1)}, u32[]{:S(2)}, u32[]{:S(2)}) collective-permute-start(bf16[384,256]{1,0:T(8,128)(2,1)} %slice.88), channel_id=1, source_target_pairs={{0,8},{8,16},{16,24},{24,0},{1,9},{9,17},{17,25},{25,1},{2,10},{10... | collective-permute-start | bytes 589832 | tf_op jit(solution)/shard_map/ppermute | solution.py:358
  83.1 41.9 %collective-permute-start.14 = (bf16[128,2048]{1,0:T(8,128)(2,1)S(1)}, bf16[128,2048]{1,0:T(8,128)(2,1)S(1)}, u32[]{:S(2)}, u32[]{:S(2)}) collective-permute-start(bf16[128,2048]{1,0:T(8,128)(2,1)S(1)} %slice.69), channel_id=1, source_target_pairs={{0,6},{2,0},{4,2},{6,4},{1,7},{3,1},{5,3},{7,5},{8,14},{10,8},{12,... | collective-permute-start | bytes 1572872 | tf_op jit(solution)/shard_map/ppermute | solution.py:359
  87.1 37.8 %collective-permute-start.13 = (bf16[128,2048]{1,0:T(8,128)(2,1)S(1)}, bf16[128,2048]{1,0:T(8,128)(2,1)S(1)}, u32[]{:S(2)}, u32[]{:S(2)}) collective-permute-start(bf16[128,2048]{1,0:T(8,128)(2,1)S(1)} %slice.68), channel_id=1, source_target_pairs={{0,2},{2,4},{4,6},{6,0},{1,3},{3,5},{5,7},{7,1},{8,10},{10,12},{12... | collective-permute-start | bytes 1572872 | tf_op jit(solution)/shard_map/ppermute | solution.py:358
  87.2 37.8 %collective-permute-start.12 = (bf16[96,2048]{1,0:T(8,128)(2,1)S(1)}, bf16[96,2048]{1,0:T(8,128)(2,1)S(1)}, u32[]{:S(2)}, u32[]{:S(2)}) collective-permute-start(bf16[96,2048]{1,0:T(8,128)(2,1)S(1)} %copy-done.11), channel_id=1, source_target_pairs={{0,6},{2,0},{4,2},{6,4},{1,7},{3,1},{5,3},{7,5},{8,14},{10,8},{12,... | collective-permute-start | bytes 1179656 | tf_op jit(solution)/shard_map/ppermute | solution.py:420
  90.4 34.6 %collective-permute-start.11 = (bf16[96,2048]{1,0:T(8,128)(2,1)S(1)}, bf16[96,2048]{1,0:T(8,128)(2,1)S(1)}, u32[]{:S(2)}, u32[]{:S(2)}) collective-permute-start(bf16[96,2048]{1,0:T(8,128)(2,1)S(1)} %copy-done.11), channel_id=1, source_target_pairs={{0,2},{2,4},{4,6},{6,0},{1,3},{3,5},{5,7},{7,1},{8,10},{10,12},{12... | collective-permute-start | bytes 1179656 | tf_op jit(solution)/shard_map/ppermute | solution.py:419
  128.8 74.7 %collective-permute-start.31 = (bf16[1024,2048]{1,0:T(8,128)(2,1)}, bf16[1024,2048]{1,0:T(8,128)(2,1)}, u32[]{:S(2)}, u32[]{:S(2)}) collective-permute-start(bf16[1024,2048]{1,0:T(8,128)(2,1)} %bitcast.32.refs_7_), channel_id=1, source_target_pairs={{0,1},{1,0},{2,3},{3,2},{4,5},{5,4},{6,7},{7,6},{8,9},{9,8},{10,11... | collective-permute-start | bytes 12582920 | tf_op jit(solution)/shard_map/ppermute | solution.py:341
  147.4 21.0 %collective-permute-start.18 = (bf16[768,256]{1,0:T(8,128)(2,1)S(1)}, bf16[768,256]{1,0:T(8,128)(2,1)S(1)}, u32[]{:S(2)}, u32[]{:S(2)}) collective-permute-start(bf16[768,256]{1,0:T(8,128)(2,1)S(1)} %get-tuple-element.55), channel_id=1, source_target_pairs={{0,8},{8,16},{16,24},{24,0},{1,9},{9,17},{17,25},{25,1},{2,10},{10... | collective-permute-start | bytes 1179656 | tf_op jit(solution)/shard_map/ppermute | solution.py:369
  147.7 20.7 %collective-permute-start.19 = (bf16[768,256]{1,0:T(8,128)(2,1)S(1)}, bf16[768,256]{1,0:T(8,128)(2,1)S(1)}, u32[]{:S(2)}, u32[]{:S(2)}) collective-permute-start(bf16[768,256]{1,0:T(8,128)(2,1)S(1)} %get-tuple-element.56), channel_id=1, source_target_pairs={{0,24},{8,0},{16,8},{24,16},{1,25},{9,1},{17,9},{25,17},{2,26},{10... | collective-permute-start | bytes 1179656 | tf_op jit(solution)/shard_map/ppermute | solution.py:370
  150.7 14.7 %collective-permute-start.20 = (bf16[384,256]{1,0:T(8,128)(2,1)S(1)}, bf16[384,256]{1,0:T(8,128)(2,1)S(1)}, u32[]{:S(2)}, u32[]{:S(2)}) collective-permute-start(bf16[384,256]{1,0:T(8,128)(2,1)S(1)} %get-tuple-element.53), channel_id=1, source_target_pairs={{0,16},{8,24},{16,0},{24,8},{1,17},{9,25},{17,1},{25,9},{2,18},{10... | collective-permute-start | bytes 589832 | tf_op jit(solution)/shard_map/ppermute | solution.py:371
  151.4 17.0 %collective-permute-start.21 = (bf16[384,256]{1,0:T(8,128)(2,1)S(1)}, bf16[384,256]{1,0:T(8,128)(2,1)S(1)}, u32[]{:S(2)}, u32[]{:S(2)}) collective-permute-start(bf16[384,256]{1,0:T(8,128)(2,1)S(1)} %get-tuple-element.54), channel_id=1, source_target_pairs={{0,16},{8,24},{16,0},{24,8},{1,17},{9,25},{17,1},{25,9},{2,18},{10... | collective-permute-start | bytes 589832 | tf_op jit(solution)/shard_map/ppermute | solution.py:372
  168.6 13.3 %collective-permute-start.22 = (bf16[768,256]{1,0:T(8,128)(2,1)S(1)}, bf16[768,256]{1,0:T(8,128)(2,1)S(1)}, u32[]{:S(2)}, u32[]{:S(2)}) collective-permute-start(bf16[768,256]{1,0:T(8,128)(2,1)S(1)} %fusion.7), channel_id=1, source_target_pairs={{0,0},{8,8},{48,16},{56,24},{64,32},{72,40},{112,48},{120,56},{96,... | collective-permute-start | bytes 1179656 | tf_op jit(solution)/shard_map/ppermute | solution.py:437
  170.6 14.6 %collective-permute-start.28 = (bf16[48,2048]{1,0:T(8,128)(2,1)S(1)}, bf16[48,2048]{1,0:T(8,128)(2,1)S(1)}, u32[]{:S(2)}, u32[]{:S(2)}) collective-permute-start(bf16[48,2048]{1,0:T(8,128)(2,1)S(1)} %slice.77), channel_id=1, source_target_pairs={{0,2},{2,4},{4,6},{6,0},{1,3},{3,5},{5,7},{7,1},{8,10},{10,12},{12... | collective-permute-start | bytes 589832 | tf_op jit(solution)/shard_map/ppermute | solution.py:358
  170.7 14.5 %collective-permute-start.29 = (bf16[48,2048]{1,0:T(8,128)(2,1)S(1)}, bf16[48,2048]{1,0:T(8,128)(2,1)S(1)}, u32[]{:S(2)}, u32[]{:S(2)}) collective-permute-start(bf16[48,2048]{1,0:T(8,128)(2,1)S(1)} %slice.78), channel_id=1, source_target_pairs={{0,6},{2,0},{4,2},{6,4},{1,7},{3,1},{5,3},{7,5},{8,14},{10,8},{12,... | collective-permute-start | bytes 589832 | tf_op jit(solution)/shard_map/ppermute | solution.py:359
  232.5 22.4 %collective-permute-start.33 = (bf16[96,2048]{1,0:T(8,128)(2,1)S(1)}, bf16[96,2048]{1,0:T(8,128)(2,1)S(1)}, u32[]{:S(2)}, u32[]{:S(2)}) collective-permute-start(bf16[96,2048]{1,0:T(8,128)(2,1)S(1)} %get-tuple-element.51), channel_id=1, source_target_pairs={{0,2},{2,4},{4,6},{6,0},{1,3},{3,5},{5,7},{7,1},{8,10},{10,12},{12... | collective-permute-start | bytes 1179656 | tf_op jit(solution)/shard_map/ppermute | solution.py:369
  232.7 22.3 %collective-permute-start.34 = (bf16[96,2048]{1,0:T(8,128)(2,1)S(1)}, bf16[96,2048]{1,0:T(8,128)(2,1)S(1)}, u32[]{:S(2)}, u32[]{:S(2)}) collective-permute-start(bf16[96,2048]{1,0:T(8,128)(2,1)S(1)} %get-tuple-element.52), channel_id=1, source_target_pairs={{0,6},{2,0},{4,2},{6,4},{1,7},{3,1},{5,3},{7,5},{8,14},{10,8},{12,... | collective-permute-start | bytes 1179656 | tf_op jit(solution)/shard_map/ppermute | solution.py:370
  236.1 15.5 %collective-permute-start.35 = (bf16[48,2048]{1,0:T(8,128)(2,1)S(1)}, bf16[48,2048]{1,0:T(8,128)(2,1)S(1)}, u32[]{:S(2)}, u32[]{:S(2)}) collective-permute-start(bf16[48,2048]{1,0:T(8,128)(2,1)S(1)} %get-tuple-element.49), channel_id=1, source_target_pairs={{0,4},{2,6},{4,0},{6,2},{1,5},{3,7},{5,1},{7,3},{8,12},{10,14},{12... | collective-permute-start | bytes 589832 | tf_op jit(solution)/shard_map/ppermute | solution.py:371
  237.5 17.4 %collective-permute-start.36 = (bf16[48,2048]{1,0:T(8,128)(2,1)S(1)}, bf16[48,2048]{1,0:T(8,128)(2,1)S(1)}, u32[]{:S(2)}, u32[]{:S(2)}) collective-permute-start(bf16[48,2048]{1,0:T(8,128)(2,1)S(1)} %get-tuple-element.50), channel_id=1, source_target_pairs={{0,4},{2,6},{4,0},{6,2},{1,5},{3,7},{5,1},{7,3},{8,12},{10,14},{12... | collective-permute-start | bytes 589832 | tf_op jit(solution)/shard_map/ppermute | solution.py:372
  (33 other events, 326.3 us)
Sparse Core Ops, SparseCore 0:
  35.0 78.9 all-gather.1
where the time goes:
time: 263 us
  waiting for transfers between devices  96.6 us (37%)
  Pallas kernels  65.1 us (25%)
  starting transfers between devices  57.8 us (22%)
  other arithmetic  16.3 us (6%)
  between operations  13.9 us (5%)
  local copies, waits for them, and re-layouts  13.1 us (5%)
    pallas_call x1, Pallas kernels, attention(): pl.pallas_call(attention_body, grid_spec=pltpu.PrefetchScalarGridSpec(num...  34.5 us
    pallas_call x1, Pallas kernels, mlp(): pl.pallas_call(mlp_body, grid_spec=pltpu.PrefetchScalarGridSpec(num_scala...  23.3 us
    ppermute x2, waiting for transfers between devices, exchanged(): top = lax.ppermute(pieces[2, :h], axis, ring(2))  23 us
    ppermute x4, starting transfers between devices, passed_on(): bottom = lax.ppermute(after[h:], axis, ring(3))  14.6 us
    ppermute x1, waiting for transfers between devices, on_device(): queries = lax.ppermute(queries, SP, balanced(False))  10.3 us
    another operation x8, other arithmetic, together(): return jnp.stack([a, after, jnp.concatenate(opposite, axis=0), before])  9.91 us
    ppermute x1, waiting for transfers between devices, on_device(): kv_before = lax.ppermute(kv, 'z', ring(1))  9.85 us
    ppermute x1, waiting for transfers between devices, on_device(): mixed = lax.ppermute(mixed, SP, balanced(True))  7.94 us
  transfers between devices with their start and end apart: 38, of which 17 were waited for; matrix products, arithmetic and copies ran while one was open for 9% of the time, Pallas kernels for 16%

commit v1 on v0

--- a/solution.py
+++ b/solution.py
@@ -413,16 +413,13 @@
     o_after = lax.ppermute(outs_in, "y", ring(3))
     offsets = kv[:, BLOCK : BLOCK + 6].reshape(4, 3, 4, LANES).astype(jnp.float32) * LOG2E
 
-    kv, queries, offsets, kinds, o_before, o_after, residual = lax.optimization_barrier(
-        (kv, queries, offsets, kinds, o_before, o_after, residual)
+    outs, totals = attention(kinds, queries, kv, offsets)
+    outs, totals, o_before, o_after, residual = lax.optimization_barrier(
+        (outs, totals, o_before, o_after, residual)
     )
     r_before = lax.ppermute(residual, "y", ring(1))
     r_after = lax.ppermute(residual, "y", ring(3))
     o_opposite = passed_on(o_before, o_after, "y")
-    outs, totals = attention(kinds, queries, kv, offsets)
-    outs, totals, r_before, r_after, o_opposite = lax.optimization_barrier(
-        (outs, totals, r_before, r_after, o_opposite)
-    )
     o_own = together(outs_in, o_before, o_after, o_opposite).reshape(1024, 2048)
     from_before = lax.ppermute(totals, "x", ring(1))
     from_after = lax.ppermute(totals, "x", ring(3))

time: 263 us -> 272 us (1.034)
  the two profiles are of different devices: /device:TPU:96 before, /device:TPU:0 now
where the time goes in v1:
time: 272 us; the launch traced here: 271 us
  waiting for transfers between devices  87.1 us (32%)
  starting transfers between devices  73.9 us (27%)
  Pallas kernels  65.1 us (24%)
  other arithmetic  16.3 us (6%)
  local copies, waits for them, and re-layouts  14.5 us (5%)
  between operations  13.9 us (5%)
    pallas_call x1, Pallas kernels, attention(): pl.pallas_call(attention_body, grid_spec=pltpu.PrefetchScalarGridSpec(num...  34.6 us
    pallas_call x1, Pallas kernels, mlp(): pl.pallas_call(mlp_body, grid_spec=pltpu.PrefetchScalarGridSpec(num_scala...  23.3 us
    ppermute x2, waiting for transfers between devices, exchanged(): top = lax.ppermute(pieces[2, :h], axis, ring(2))  23 us
    ppermute x1, starting transfers between devices, on_device(): q_after = lax.ppermute(queries, 'x', ring(3))  17.2 us
    ppermute x4, starting transfers between devices, passed_on(): bottom = lax.ppermute(after[h:], axis, ring(3))  15.4 us
    another operation x8, other arithmetic, together(): return jnp.stack([a, after, jnp.concatenate(opposite, axis=0), before])  9.94 us
    ppermute x4, waiting for transfers between devices, passed_on(): top = lax.ppermute(before[:h], axis, ring(1))  8.75 us
    ppermute x1, waiting for transfers between devices, on_device(): kv_before = lax.ppermute(kv, 'z', ring(1))  8.38 us
  transfers between devices with their start and end apart: 38, of which 21 were waited for; matrix products, arithmetic and copies ran while one was open for 8% of the time, Pallas kernels for 15%

profile of v1, /device:TPU:0, one launch (start us, length us, event | category | flops | bytes accessed | tf_op | source)
XLA Modules:
  0.0 270.8 jit_solution(11752155656377524687)
XLA Ops:
  11.1 17.2 %collective-permute-start.1 = (bf16[768,256]{1,0:T(8,128)(2,1)S(1)}, bf16[768,256]{1,0:T(8,128)(2,1)S(1)}, u32[]{:S(2)}, u32[]{:S(2)}) collective-permute-start(bf16[768,256]{1,0:T(8,128)(2,1)S(1)} %collective-permute-done), channel_id=1, source_target_pairs={{0,24},{8,0},{16,8},{24,16},{1,25},{9,1},{17,9},{25,17},{2,26},{10... | collective-permute-start | bytes 1179656 | tf_op jit(solution)/shard_map/ppermute | solution.py:405
  29.8 6.2 %collective-permute-done.1 = bf16[768,256]{1,0:T(8,128)(2,1)S(1)} collective-permute-done((bf16[768,256]{1,0:T(8,128)(2,1)S(1)}, bf16[768,256]{1,0:T(8,128)(2,1)S(1)}, u32[]{:S(2)}, u32[]{:S(2)}) %collective-permute-start.1) | collective-permute-done | bytes 393248 | tf_op jit(solution)/shard_map/ppermute | solution.py:405
  47.2 3.3 %collective-permute-done.2 = bf16[768,256]{1,0:T(8,128)(2,1)S(1)} collective-permute-done((bf16[768,256]{1,0:T(8,128)(2,1)}, bf16[768,256]{1,0:T(8,128)(2,1)S(1)}, u32[]{:S(2)}, u32[]{:S(2)}) %collective-permute-start.2) | collective-permute-done | bytes 393248 | tf_op jit(solution)/shard_map/ppermute | solution.py:404
  51.9 8.4 %collective-permute-done.6 = bf16[784,512]{1,0:T(8,128)(2,1)S(1)} collective-permute-done((bf16[784,512]{1,0:T(8,128)(2,1)S(1)}, bf16[784,512]{1,0:T(8,128)(2,1)S(1)}, u32[]{:S(2)}, u32[]{:S(2)}) %collective-permute-start.6) | collective-permute-done | bytes 802848 | tf_op jit(solution)/shard_map/ppermute | solution.py:401
  60.2 6.0 %collective-permute-start.4 = (bf16[384,256]{1,0:T(8,128)(2,1)S(1)}, bf16[384,256]{1,0:T(8,128)(2,1)}, u32[]{:S(2)}, u32[]{:S(2)}) collective-permute-start(bf16[384,256]{1,0:T(8,128)(2,1)S(1)} %slice.64), channel_id=1, source_target_pairs={{0,24},{8,0},{16,8},{24,16},{1,25},{9,1},{17,9},{25,17},{2,26},{10... | collective-permute-start | bytes 589832 | tf_op jit(solution)/shard_map/ppermute | solution.py:359
  67.9 3.2 %collective-permute-start.8 = (bf16[392,512]{1,0:T(8,128)(2,1)}, bf16[392,512]{1,0:T(8,128)(2,1)}, u32[]{:S(2)}, u32[]{:S(2)}) collective-permute-start(bf16[392,512]{1,0:T(8,128)(2,1)} %slice.88), channel_id=1, source_target_pairs={{0,96},{32,0},{64,32},{96,64},{1,97},{33,1},{65,33},{97,65},{2,98}... | collective-permute-start | bytes 1204232 | tf_op jit(solution)/shard_map/ppermute | solution.py:359
  82.6 34.6 %stick_attention.1 = (bf16[16,768,256]{2,1,0:T(8,128)(2,1)S(1)}, f32[48,768]{1,0:T(8,128)S(1)}) custom-call(s32[16]{0:T(128)S(1)} %add.124.table, bf16[4,768,256]{2,1,0:T(8,128)(2,1)S(1)} %copy-done, bf16[4,784,512]{2,1,0:T(8,128)(2,1)S(1)} %pad_maximum_fusion.1.kv_ref, f32[4,3,4,256]{3,2,1,0:T(4,128)S(1)} %mul.26.off_ref, bf16[256,256]{1,0:T(8,128)(2,1)S(1)} %copy-done.1), custom_call_target="tpu_custom_call" | custom-call | tf_op jit(solution)/shard_map/stick_attention/pallas_call | solution.py:115
  123.7 7.1 %collective-permute-done.29 = bf16[128,2048]{1,0:T(8,128)(2,1)S(1)} collective-permute-done((bf16[128,2048]{1,0:T(8,128)(2,1)S(1)}, bf16[128,2048]{1,0:T(8,128)(2,1)S(1)}, u32[]{:S(2)}, u32[]{:S(2)}) %collective-permute-start.29) | collective-permute-done | bytes 524320 | tf_op jit(solution)/shard_map/ppermute | solution.py:358
  130.8 3.7 %pad_maximum_fusion = bf16[4,256,2048]{2,1,0:T(8,128)(2,1)} fusion(bf16[1,256,2048]{2,1,0:T(8,128)(2,1)} %bitcast.31, bf16[1,256,2048]{2,1,0:T(8,128)(2,1)S(1)} %maximum_bitcast_fusion, bf16[1,256,2048]{2,1,0:T(8,128)(2,1)} %bitcast.29, bf16[1,256,2048]{2,1,0:T(8,128)(2,1)} %bitcast.28), kind=kLoop, calls=%fused_computation.1 | loop fusion | flops 6291456 | bytes 8388608 | tf_op jit(solution)/shard_map/stack | solution.py:364
  134.7 3.1 %collective-permute-start.11 = (f32[48,768]{1,0:T(8,128)S(1)}, f32[48,768]{1,0:T(8,128)S(1)}, u32[]{:S(2)}, u32[]{:S(2)}) collective-permute-start(f32[48,768]{1,0:T(8,128)S(1)} %get-tuple-element.25.t0), channel_id=1, source_target_pairs={{0,24},{8,0},{16,8},{24,16},{1,25},{9,1},{17,9},{25,17},{2,26},{10... | collective-permute-start | bytes 442376 | tf_op jit(solution)/shard_map/ppermute | solution.py:425
  137.9 7.3 %collective-permute-done.13.t3 = f32[48,768]{1,0:T(8,128)S(1)} collective-permute-done((f32[48,768]{1,0:T(8,128)S(1)}, f32[48,768]{1,0:T(8,128)S(1)}, u32[]{:S(2)}, u32[]{:S(2)}) %collective-permute-start.13) | collective-permute-done | bytes 147488 | tf_op jit(solution)/shard_map/ppermute | solution.py:424
  145.8 7.3 %combine_key_blocks.1 = bf16[4,768,256]{2,1,0:T(8,128)(2,1)S(1)} custom-call(s32[2]{0:T(128)S(1)} %pad_add_fusion.1.place, bf16[16,768,256]{2,1,0:T(8,128)(2,1)S(1)} %get-tuple-element.24.outs, f32[48,768]{1,0:T(8,128)S(1)} %get-tuple-element.25.t0, f32[48,768]{1,0:T(8,128)S(1)} %collective-permute-done.11.t1, f32[48,768]{1,0:T(8,128)S(1)} %collective-permute-done.12.t2, ...), custom_call_target="tpu_custom_call" | custom-call | tf_op jit(solution)/shard_map/combine_key_blocks/pallas_call | solution.py:185
  160.1 11.1 %collective-permute-done.16 = bf16[384,256]{1,0:T(8,128)(2,1)S(1)} collective-permute-done((bf16[384,256]{1,0:T(8,128)(2,1)S(1)}, bf16[384,256]{1,0:T(8,128)(2,1)S(1)}, u32[]{:S(2)}, u32[]{:S(2)}) %collective-permute-start.16) | collective-permute-done | bytes 196640 | tf_op jit(solution)/shard_map/ppermute | solution.py:371
  174.2 3.3 %collective-permute-start.24 = (bf16[96,2048]{1,0:T(8,128)(2,1)S(1)}, bf16[96,2048]{1,0:T(8,128)(2,1)S(1)}, u32[]{:S(2)}, u32[]{:S(2)}) collective-permute-start(bf16[96,2048]{1,0:T(8,128)(2,1)S(1)} %copy-done.11), channel_id=1, source_target_pairs={{0,6},{2,0},{4,2},{6,4},{1,7},{3,1},{5,3},{7,5},{8,14},{10,8},{12,... | collective-permute-start | bytes 1179656 | tf_op jit(solution)/shard_map/ppermute | solution.py:421
  181.8 3.1 %collective-permute-done.24 = bf16[96,2048]{1,0:T(8,128)(2,1)S(1)} collective-permute-done((bf16[96,2048]{1,0:T(8,128)(2,1)S(1)}, bf16[96,2048]{1,0:T(8,128)(2,1)S(1)}, u32[]{:S(2)}, u32[]{:S(2)}) %collective-permute-start.24) | collective-permute-done | bytes 393248 | tf_op jit(solution)/shard_map/ppermute | solution.py:421
  184.9 3.8 %collective-permute-start.27 = (bf16[48,2048]{1,0:T(8,128)(2,1)S(1)}, bf16[48,2048]{1,0:T(8,128)(2,1)S(1)}, u32[]{:S(2)}, u32[]{:S(2)}) collective-permute-start(bf16[48,2048]{1,0:T(8,128)(2,1)S(1)} %slice.98), channel_id=1, source_target_pairs={{0,6},{2,0},{4,2},{6,4},{1,7},{3,1},{5,3},{7,5},{8,14},{10,8},{12,... | collective-permute-start | bytes 589832 | tf_op jit(solution)/shard_map/ppermute | solution.py:359
  188.7 3.2 %collective-permute-start.19 = (bf16[768,256]{1,0:T(8,128)(2,1)S(1)}, bf16[768,256]{1,0:T(8,128)(2,1)S(1)}, u32[]{:S(2)}, u32[]{:S(2)}) collective-permute-start(bf16[768,256]{1,0:T(8,128)(2,1)S(1)} %collective-permute-done.18), channel_id=1, source_target_pairs={{0,6},{2,0},{4,2},{6,4},{1,7},{3,1},{5,3},{7,5},{8,14},{10,8},{12,... | collective-permute-start | bytes 1179656 | tf_op jit(solution)/shard_map/ppermute | solution.py:347
  194.0 4.6 %collective-permute-done.20 = bf16[768,256]{1,0:T(8,128)(2,1)S(1)} collective-permute-done((bf16[768,256]{1,0:T(8,128)(2,1)S(1)}, bf16[768,256]{1,0:T(8,128)(2,1)S(1)}, u32[]{:S(2)}, u32[]{:S(2)}) %collective-permute-start.20) | collective-permute-done | bytes 393248 | tf_op jit(solution)/shard_map/ppermute | solution.py:346
  200.0 3.8 %collective-permute-start.22 = (bf16[384,256]{1,0:T(8,128)(2,1)S(1)}, bf16[384,256]{1,0:T(8,128)(2,1)S(1)}, u32[]{:S(2)}, u32[]{:S(2)}) collective-permute-start(bf16[384,256]{1,0:T(8,128)(2,1)S(1)} %slice.96), channel_id=1, source_target_pairs={{0,6},{2,0},{4,2},{6,4},{1,7},{3,1},{5,3},{7,5},{8,14},{10,8},{12,... | collective-permute-start | bytes 589832 | tf_op jit(solution)/shard_map/ppermute | solution.py:349
  211.1 23.3 %project_norm_mlp.1 = (f32[96,2048]{1,0:T(8,128)}, bf16[4,96,2048]{2,1,0:T(8,128)(2,1)}, bf16[4,96,2048]{2,1,0:T(8,128)(2,1)}) custom-call(s32[2]{0:T(128)} %pad_add_fusion.place, bf16[4,192,1024]{2,1,0:T(8,128)(2,1)} %bitcast.61, bf16[4,192,1024]{2,1,0:T(8,128)(2,1)} %bitcast.62, bf16[4,192,1024]{2,1,0:T(8,128)(2,1)} %bitcast.23.refs_2_.refs_3_, ...), custom_call_target="tpu_custom_call" | custom-call | tf_op jit(solution)/shard_map/project_norm_mlp/pallas_call | solution.py:294
  234.6 3.5 %collective-permute-done.32 = bf16[4,96,2048]{2,1,0:T(8,128)(2,1)S(1)} collective-permute-done((bf16[4,96,2048]{2,1,0:T(8,128)(2,1)}, bf16[4,96,2048]{2,1,0:T(8,128)(2,1)S(1)}, u32[]{:S(2)}, u32[]{:S(2)}) %collective-permute-start.32) | collective-permute-done | bytes 1572896 | tf_op jit(solution)/shard_map/ppermute | solution.py:341
  240.2 3.8 %collective-permute-start.34 = (bf16[96,2048]{1,0:T(8,128)(2,1)S(1)}, bf16[96,2048]{1,0:T(8,128)(2,1)S(1)}, u32[]{:S(2)}, u32[]{:S(2)}) collective-permute-start(bf16[96,2048]{1,0:T(8,128)(2,1)S(1)} %get-tuple-element.36), channel_id=1, source_target_pairs={{0,6},{2,0},{4,2},{6,4},{1,7},{3,1},{5,3},{7,5},{8,14},{10,8},{12,... | collective-permute-start | bytes 1179656 | tf_op jit(solution)/shard_map/ppermute | solution.py:370
  247.7 11.9 %collective-permute-done.35 = bf16[48,2048]{1,0:T(8,128)(2,1)S(1)} collective-permute-done((bf16[48,2048]{1,0:T(8,128)(2,1)S(1)}, bf16[48,2048]{1,0:T(8,128)(2,1)S(1)}, u32[]{:S(2)}, u32[]{:S(2)}) %collective-permute-start.35) | collective-permute-done | bytes 196640 | tf_op jit(solution)/shard_map/ppermute | solution.py:371
  259.6 3.4 %collective-permute-done.36 = bf16[48,2048]{1,0:T(8,128)(2,1)S(1)} collective-permute-done((bf16[48,2048]{1,0:T(8,128)(2,1)S(1)}, bf16[48,2048]{1,0:T(8,128)(2,1)S(1)}, u32[]{:S(2)}, u32[]{:S(2)}) %collective-permute-start.36) | collective-permute-done | bytes 196640 | tf_op jit(solution)/shard_map/ppermute | solution.py:372
  (148 shorter events, 70.8 us)
Async XLA Ops:
  6.5 204.5 %all-gather.2.cloned.1.call-start = ((), (), s32[]{:S(2)}) async-start(), calls=%async_computation | async-start | bytes 9469952 | tf_op jit(solution)/shard_map/all_gather | solution.py:408
  11.1 25.0 %collective-permute-start.1 = (bf16[768,256]{1,0:T(8,128)(2,1)S(1)}, bf16[768,256]{1,0:T(8,128)(2,1)S(1)}, u32[]{:S(2)}, u32[]{:S(2)}) collective-permute-start(bf16[768,256]{1,0:T(8,128)(2,1)S(1)} %collective-permute-done), channel_id=1, source_target_pairs={{0,24},{8,0},{16,8},{24,16},{1,25},{9,1},{17,9},{25,17},{2,26},{10... | collective-permute-start | bytes 1179656 | tf_op jit(solution)/shard_map/ppermute | solution.py:405
  36.1 24.1 %collective-permute-start.6 = (bf16[784,512]{1,0:T(8,128)(2,1)S(1)}, bf16[784,512]{1,0:T(8,128)(2,1)S(1)}, u32[]{:S(2)}, u32[]{:S(2)}) collective-permute-start(bf16[784,512]{1,0:T(8,128)(2,1)S(1)} %fusion.1), channel_id=1, source_target_pairs={{0,32},{32,64},{64,96},{96,0},{1,33},{33,65},{65,97},{97,1},{2,34}... | collective-permute-start | bytes 2408456 | tf_op jit(solution)/shard_map/ppermute | solution.py:401
  36.8 30.3 %collective-permute-start.5 = (bf16[784,512]{1,0:T(8,128)(2,1)S(1)}, bf16[784,512]{1,0:T(8,128)(2,1)S(1)}, u32[]{:S(2)}, u32[]{:S(2)}) collective-permute-start(bf16[784,512]{1,0:T(8,128)(2,1)S(1)} %fusion.1), channel_id=1, source_target_pairs={{0,96},{32,0},{64,32},{96,64},{1,97},{33,1},{65,33},{97,65},{2,98}... | collective-permute-start | bytes 2408456 | tf_op jit(solution)/shard_map/ppermute | solution.py:402
  39.4 11.0 %collective-permute-start.2 = (bf16[768,256]{1,0:T(8,128)(2,1)}, bf16[768,256]{1,0:T(8,128)(2,1)S(1)}, u32[]{:S(2)}, u32[]{:S(2)}) collective-permute-start(bf16[768,256]{1,0:T(8,128)(2,1)} %copy-done.12), channel_id=1, source_target_pairs={{0,8},{8,16},{16,24},{24,0},{1,9},{9,17},{17,25},{25,1},{2,10},{10... | collective-permute-start | bytes 1179656 | tf_op jit(solution)/shard_map/ppermute | solution.py:404
  44.2 73.0 %collective-permute-start.10 = (bf16[256,2048]{1,0:T(8,128)(2,1)}, bf16[256,2048]{1,0:T(8,128)(2,1)}, u32[]{:S(2)}, u32[]{:S(2)}) collective-permute-start(bf16[256,2048]{1,0:T(8,128)(2,1)} %constant_dynamic-update-slice_fusion), channel_id=1, source_target_pairs={{0,6},{2,0},{4,2},{6,4},{1,7},{3,1},{5,3},{7,5},{8,14},{10,8},{12,... | collective-permute-start | bytes 3145736 | tf_op jit(solution)/shard_map/ppermute | solution.py:413
  47.2 70.0 %collective-permute-start.9 = (bf16[256,2048]{1,0:T(8,128)(2,1)}, bf16[256,2048]{1,0:T(8,128)(2,1)}, u32[]{:S(2)}, u32[]{:S(2)}) collective-permute-start(bf16[256,2048]{1,0:T(8,128)(2,1)} %constant_dynamic-update-slice_fusion), channel_id=1, source_target_pairs={{0,2},{2,4},{4,6},{6,0},{1,3},{3,5},{5,7},{7,1},{8,10},{10,12},{12... | collective-permute-start | bytes 3145736 | tf_op jit(solution)/shard_map/ppermute | solution.py:412
  51.2 16.7 %collective-permute-start.3 = (bf16[384,256]{1,0:T(8,128)(2,1)}, bf16[384,256]{1,0:T(8,128)(2,1)}, u32[]{:S(2)}, u32[]{:S(2)}) collective-permute-start(bf16[384,256]{1,0:T(8,128)(2,1)} %slice.86), channel_id=1, source_target_pairs={{0,8},{8,16},{16,24},{24,0},{1,9},{9,17},{17,25},{25,1},{2,10},{10... | collective-permute-start | bytes 589832 | tf_op jit(solution)/shard_map/ppermute | solution.py:358
  60.2 11.0 %collective-permute-start.4 = (bf16[384,256]{1,0:T(8,128)(2,1)S(1)}, bf16[384,256]{1,0:T(8,128)(2,1)}, u32[]{:S(2)}, u32[]{:S(2)}) collective-permute-start(bf16[384,256]{1,0:T(8,128)(2,1)S(1)} %slice.64), channel_id=1, source_target_pairs={{0,24},{8,0},{16,8},{24,16},{1,25},{9,1},{17,9},{25,17},{2,26},{10... | collective-permute-start | bytes 589832 | tf_op jit(solution)/shard_map/ppermute | solution.py:359
  67.9 10.7 %collective-permute-start.8 = (bf16[392,512]{1,0:T(8,128)(2,1)}, bf16[392,512]{1,0:T(8,128)(2,1)}, u32[]{:S(2)}, u32[]{:S(2)}) collective-permute-start(bf16[392,512]{1,0:T(8,128)(2,1)} %slice.88), channel_id=1, source_target_pairs={{0,96},{32,0},{64,32},{96,64},{1,97},{33,1},{65,33},{97,65},{2,98}... | collective-permute-start | bytes 1204232 | tf_op jit(solution)/shard_map/ppermute | solution.py:359
  119.3 11.4 %collective-permute-start.29 = (bf16[128,2048]{1,0:T(8,128)(2,1)S(1)}, bf16[128,2048]{1,0:T(8,128)(2,1)S(1)}, u32[]{:S(2)}, u32[]{:S(2)}) collective-permute-start(bf16[128,2048]{1,0:T(8,128)(2,1)S(1)} %slice.77), channel_id=1, source_target_pairs={{0,2},{2,4},{4,6},{6,0},{1,3},{3,5},{5,7},{7,1},{8,10},{10,12},{12... | collective-permute-start | bytes 1572872 | tf_op jit(solution)/shard_map/ppermute | solution.py:358
  134.6 76.5 %collective-permute-start.31 = (bf16[1024,2048]{1,0:T(8,128)(2,1)}, bf16[1024,2048]{1,0:T(8,128)(2,1)}, u32[]{:S(2)}, u32[]{:S(2)}) collective-permute-start(bf16[1024,2048]{1,0:T(8,128)(2,1)} %bitcast.32.refs_7_), channel_id=1, source_target_pairs={{0,1},{1,0},{2,3},{3,2},{4,5},{5,4},{6,7},{7,6},{8,9},{9,8},{10,11... | collective-permute-start | bytes 12582920 | tf_op jit(solution)/shard_map/ppermute | solution.py:341
  134.7 11.2 %collective-permute-start.11 = (f32[48,768]{1,0:T(8,128)S(1)}, f32[48,768]{1,0:T(8,128)S(1)}, u32[]{:S(2)}, u32[]{:S(2)}) collective-permute-start(f32[48,768]{1,0:T(8,128)S(1)} %get-tuple-element.25.t0), channel_id=1, source_target_pairs={{0,24},{8,0},{16,8},{24,16},{1,25},{9,1},{17,9},{25,17},{2,26},{10... | collective-permute-start | bytes 442376 | tf_op jit(solution)/shard_map/ppermute | solution.py:425
  153.2 24.3 %collective-permute-start.14 = (bf16[768,256]{1,0:T(8,128)(2,1)S(1)}, bf16[768,256]{1,0:T(8,128)(2,1)S(1)}, u32[]{:S(2)}, u32[]{:S(2)}) collective-permute-start(bf16[768,256]{1,0:T(8,128)(2,1)S(1)} %get-tuple-element.39), channel_id=1, source_target_pairs={{0,8},{8,16},{16,24},{24,0},{1,9},{9,17},{17,25},{25,1},{2,10},{10... | collective-permute-start | bytes 1179656 | tf_op jit(solution)/shard_map/ppermute | solution.py:369
  153.5 24.0 %collective-permute-start.15 = (bf16[768,256]{1,0:T(8,128)(2,1)S(1)}, bf16[768,256]{1,0:T(8,128)(2,1)S(1)}, u32[]{:S(2)}, u32[]{:S(2)}) collective-permute-start(bf16[768,256]{1,0:T(8,128)(2,1)S(1)} %get-tuple-element.40), channel_id=1, source_target_pairs={{0,24},{8,0},{16,8},{24,16},{1,25},{9,1},{17,9},{25,17},{2,26},{10... | collective-permute-start | bytes 1179656 | tf_op jit(solution)/shard_map/ppermute | solution.py:370
  156.5 14.7 %collective-permute-start.16 = (bf16[384,256]{1,0:T(8,128)(2,1)S(1)}, bf16[384,256]{1,0:T(8,128)(2,1)S(1)}, u32[]{:S(2)}, u32[]{:S(2)}) collective-permute-start(bf16[384,256]{1,0:T(8,128)(2,1)S(1)} %get-tuple-element.37), channel_id=1, source_target_pairs={{0,16},{8,24},{16,0},{24,8},{1,17},{9,25},{17,1},{25,9},{2,18},{10... | collective-permute-start | bytes 589832 | tf_op jit(solution)/shard_map/ppermute | solution.py:371
  157.2 17.0 %collective-permute-start.17 = (bf16[384,256]{1,0:T(8,128)(2,1)S(1)}, bf16[384,256]{1,0:T(8,128)(2,1)S(1)}, u32[]{:S(2)}, u32[]{:S(2)}) collective-permute-start(bf16[384,256]{1,0:T(8,128)(2,1)S(1)} %get-tuple-element.38), channel_id=1, source_target_pairs={{0,16},{8,24},{16,0},{24,8},{1,17},{9,25},{17,1},{25,9},{2,18},{10... | collective-permute-start | bytes 589832 | tf_op jit(solution)/shard_map/ppermute | solution.py:372
  174.2 10.7 %collective-permute-start.24 = (bf16[96,2048]{1,0:T(8,128)(2,1)S(1)}, bf16[96,2048]{1,0:T(8,128)(2,1)S(1)}, u32[]{:S(2)}, u32[]{:S(2)}) collective-permute-start(bf16[96,2048]{1,0:T(8,128)(2,1)S(1)} %copy-done.11), channel_id=1, source_target_pairs={{0,6},{2,0},{4,2},{6,4},{1,7},{3,1},{5,3},{7,5},{8,14},{10,8},{12,... | collective-permute-start | bytes 1179656 | tf_op jit(solution)/shard_map/ppermute | solution.py:421
  177.7 11.0 %collective-permute-start.18 = (bf16[768,256]{1,0:T(8,128)(2,1)S(1)}, bf16[768,256]{1,0:T(8,128)(2,1)S(1)}, u32[]{:S(2)}, u32[]{:S(2)}) collective-permute-start(bf16[768,256]{1,0:T(8,128)(2,1)S(1)} %fusion.7), channel_id=1, source_target_pairs={{0,0},{8,8},{48,16},{56,24},{64,32},{72,40},{112,48},{120,56},{96,... | collective-permute-start | bytes 1179656 | tf_op jit(solution)/shard_map/ppermute | solution.py:434
  188.7 11.3 %collective-permute-start.19 = (bf16[768,256]{1,0:T(8,128)(2,1)S(1)}, bf16[768,256]{1,0:T(8,128)(2,1)S(1)}, u32[]{:S(2)}, u32[]{:S(2)}) collective-permute-start(bf16[768,256]{1,0:T(8,128)(2,1)S(1)} %collective-permute-done.18), channel_id=1, source_target_pairs={{0,6},{2,0},{4,2},{6,4},{1,7},{3,1},{5,3},{7,5},{8,14},{10,8},{12,... | collective-permute-start | bytes 1179656 | tf_op jit(solution)/shard_map/ppermute | solution.py:347
  240.2 22.8 %collective-permute-start.33 = (bf16[96,2048]{1,0:T(8,128)(2,1)S(1)}, bf16[96,2048]{1,0:T(8,128)(2,1)S(1)}, u32[]{:S(2)}, u32[]{:S(2)}) collective-permute-start(bf16[96,2048]{1,0:T(8,128)(2,1)S(1)} %get-tuple-element.35), channel_id=1, source_target_pairs={{0,2},{2,4},{4,6},{6,0},{1,3},{3,5},{5,7},{7,1},{8,10},{10,12},{12... | collective-permute-start | bytes 1179656 | tf_op jit(solution)/shard_map/ppermute | solution.py:369
  240.2 22.7 %collective-permute-start.34 = (bf16[96,2048]{1,0:T(8,128)(2,1)S(1)}, bf16[96,2048]{1,0:T(8,128)(2,1)S(1)}, u32[]{:S(2)}, u32[]{:S(2)}) collective-permute-start(bf16[96,2048]{1,0:T(8,128)(2,1)S(1)} %get-tuple-element.36), channel_id=1, source_target_pairs={{0,6},{2,0},{4,2},{6,4},{1,7},{3,1},{5,3},{7,5},{8,14},{10,8},{12,... | collective-permute-start | bytes 1179656 | tf_op jit(solution)/shard_map/ppermute | solution.py:370
  244.0 15.5 %collective-permute-start.35 = (bf16[48,2048]{1,0:T(8,128)(2,1)S(1)}, bf16[48,2048]{1,0:T(8,128)(2,1)S(1)}, u32[]{:S(2)}, u32[]{:S(2)}) collective-permute-start(bf16[48,2048]{1,0:T(8,128)(2,1)S(1)} %get-tuple-element.33), channel_id=1, source_target_pairs={{0,4},{2,6},{4,0},{6,2},{1,5},{3,7},{5,1},{7,3},{8,12},{10,14},{12... | collective-permute-start | bytes 589832 | tf_op jit(solution)/shard_map/ppermute | solution.py:371
  245.5 17.4 %collective-permute-start.36 = (bf16[48,2048]{1,0:T(8,128)(2,1)S(1)}, bf16[48,2048]{1,0:T(8,128)(2,1)S(1)}, u32[]{:S(2)}, u32[]{:S(2)}) collective-permute-start(bf16[48,2048]{1,0:T(8,128)(2,1)S(1)} %get-tuple-element.34), channel_id=1, source_target_pairs={{0,4},{2,6},{4,0},{6,2},{1,5},{3,7},{5,1},{7,3},{8,12},{10,14},{12... | collective-permute-start | bytes 589832 | tf_op jit(solution)/shard_map/ppermute | solution.py:372
  (33 other events, 327.2 us)
Sparse Core Ops, SparseCore 0:
  36.2 79.2 all-gather.1

commit v2 on v1

--- a/solution.py
+++ b/solution.py
@@ -245,8 +245,8 @@
 
     @pl.when(step == 0)
     def _():
-        for copy in copies:
-            copy.start()
+        copies[0].start()
+        copies[1].start()
 
     rows[:192, :1024] = ma[0]
     rows[192:, :1024] = mb[0]
@@ -256,9 +256,15 @@
     @pl.when(step == 0)
     def _():
         copies[0].wait()
+        copies[2].start()
+
+    part = jnp.dot(rows[:, :1024], out_w[:1024], preferred_element_type=jnp.float32)
+
+    @pl.when(step == 0)
+    def _():
         copies[1].wait()
 
-    part = jnp.dot(rows[...], out_w[...], preferred_element_type=jnp.float32)
+    part = part + jnp.dot(rows[:, 1024:], out_w[1024:], preferred_element_type=jnp.float32)
     attended = part.astype(jnp.bfloat16).astype(jnp.float32)
     kept = []
     for k in range(2):

time: 272 us -> 272 us (level)
  no operation moved by 1% of the time
where the time goes in v2:
time: 272 us; the launch traced here: 271 us
  waiting for transfers between devices  87.1 us (32%)
  starting transfers between devices  74 us (27%)
  Pallas kernels  65.6 us (24%)
  other arithmetic  16.3 us (6%)
  local copies, waits for them, and re-layouts  14.5 us (5%)
  between operations  13.9 us (5%)
    pallas_call x1, Pallas kernels, attention(): pl.pallas_call(attention_body, grid_spec=pltpu.PrefetchScalarGridSpec(num...  34.6 us
    pallas_call x1, Pallas kernels, mlp(): pl.pallas_call(mlp_body, grid_spec=pltpu.PrefetchScalarGridSpec(num_scala...  23.8 us
    ppermute x2, waiting for transfers between devices, exchanged(): top = lax.ppermute(pieces[2, :h], axis, ring(2))  23 us
    ppermute x1, starting transfers between devices, on_device(): q_after = lax.ppermute(queries, 'x', ring(3))  17.2 us
    ppermute x4, starting transfers between devices, passed_on(): bottom = lax.ppermute(after[h:], axis, ring(3))  15.4 us
    another operation x8, other arithmetic, together(): return jnp.stack([a, after, jnp.concatenate(opposite, axis=0), before])  9.94 us
    ppermute x4, waiting for transfers between devices, passed_on(): top = lax.ppermute(before[:h], axis, ring(1))  8.75 us
    ppermute x1, waiting for transfers between devices, on_device(): kv_before = lax.ppermute(kv, 'z', ring(1))  8.38 us
  transfers between devices with their start and end apart: 38, of which 21 were waited for; matrix products, arithmetic and copies ran while one was open for 8% of the time, Pallas kernels for 15%

profile of v2, /device:TPU:0, one launch (start us, length us, event | category | flops | bytes accessed | tf_op | source)
XLA Modules:
  0.0 271.3 jit_solution(18358933743808404212)
XLA Ops:
  11.1 17.2 %collective-permute-start.1 = (bf16[768,256]{1,0:T(8,128)(2,1)S(1)}, bf16[768,256]{1,0:T(8,128)(2,1)S(1)}, u32[]{:S(2)}, u32[]{:S(2)}) collective-permute-start(bf16[768,256]{1,0:T(8,128)(2,1)S(1)} %collective-permute-done), channel_id=1, source_target_pairs={{0,24},{8,0},{16,8},{24,16},{1,25},{9,1},{17,9},{25,17},{2,26},{10... | collective-permute-start | bytes 1179656 | tf_op jit(solution)/shard_map/ppermute | solution.py:411
  29.8 6.2 %collective-permute-done.1 = bf16[768,256]{1,0:T(8,128)(2,1)S(1)} collective-permute-done((bf16[768,256]{1,0:T(8,128)(2,1)S(1)}, bf16[768,256]{1,0:T(8,128)(2,1)S(1)}, u32[]{:S(2)}, u32[]{:S(2)}) %collective-permute-start.1) | collective-permute-done | bytes 393248 | tf_op jit(solution)/shard_map/ppermute | solution.py:411
  47.2 3.3 %collective-permute-done.2 = bf16[768,256]{1,0:T(8,128)(2,1)S(1)} collective-permute-done((bf16[768,256]{1,0:T(8,128)(2,1)}, bf16[768,256]{1,0:T(8,128)(2,1)S(1)}, u32[]{:S(2)}, u32[]{:S(2)}) %collective-permute-start.2) | collective-permute-done | bytes 393248 | tf_op jit(solution)/shard_map/ppermute | solution.py:410
  51.9 8.4 %collective-permute-done.6 = bf16[784,512]{1,0:T(8,128)(2,1)S(1)} collective-permute-done((bf16[784,512]{1,0:T(8,128)(2,1)S(1)}, bf16[784,512]{1,0:T(8,128)(2,1)S(1)}, u32[]{:S(2)}, u32[]{:S(2)}) %collective-permute-start.6) | collective-permute-done | bytes 802848 | tf_op jit(solution)/shard_map/ppermute | solution.py:407
  60.2 6.0 %collective-permute-start.4 = (bf16[384,256]{1,0:T(8,128)(2,1)S(1)}, bf16[384,256]{1,0:T(8,128)(2,1)}, u32[]{:S(2)}, u32[]{:S(2)}) collective-permute-start(bf16[384,256]{1,0:T(8,128)(2,1)S(1)} %slice.64), channel_id=1, source_target_pairs={{0,24},{8,0},{16,8},{24,16},{1,25},{9,1},{17,9},{25,17},{2,26},{10... | collective-permute-start | bytes 589832 | tf_op jit(solution)/shard_map/ppermute | solution.py:365
  67.9 3.2 %collective-permute-start.8 = (bf16[392,512]{1,0:T(8,128)(2,1)}, bf16[392,512]{1,0:T(8,128)(2,1)}, u32[]{:S(2)}, u32[]{:S(2)}) collective-permute-start(bf16[392,512]{1,0:T(8,128)(2,1)} %slice.88), channel_id=1, source_target_pairs={{0,96},{32,0},{64,32},{96,64},{1,97},{33,1},{65,33},{97,65},{2,98}... | collective-permute-start | bytes 1204232 | tf_op jit(solution)/shard_map/ppermute | solution.py:365
  82.6 34.6 %stick_attention.1 = (bf16[16,768,256]{2,1,0:T(8,128)(2,1)S(1)}, f32[48,768]{1,0:T(8,128)S(1)}) custom-call(s32[16]{0:T(128)S(1)} %add.124.table, bf16[4,768,256]{2,1,0:T(8,128)(2,1)S(1)} %copy-done, bf16[4,784,512]{2,1,0:T(8,128)(2,1)S(1)} %pad_maximum_fusion.1.kv_ref, f32[4,3,4,256]{3,2,1,0:T(4,128)S(1)} %mul.26.off_ref, bf16[256,256]{1,0:T(8,128)(2,1)S(1)} %copy-done.1), custom_call_target="tpu_custom_call" | custom-call | tf_op jit(solution)/shard_map/stick_attention/pallas_call | solution.py:115
  123.7 7.1 %collective-permute-done.29 = bf16[128,2048]{1,0:T(8,128)(2,1)S(1)} collective-permute-done((bf16[128,2048]{1,0:T(8,128)(2,1)S(1)}, bf16[128,2048]{1,0:T(8,128)(2,1)S(1)}, u32[]{:S(2)}, u32[]{:S(2)}) %collective-permute-start.29) | collective-permute-done | bytes 524320 | tf_op jit(solution)/shard_map/ppermute | solution.py:364
  130.8 3.7 %pad_maximum_fusion = bf16[4,256,2048]{2,1,0:T(8,128)(2,1)} fusion(bf16[1,256,2048]{2,1,0:T(8,128)(2,1)} %bitcast.31, bf16[1,256,2048]{2,1,0:T(8,128)(2,1)S(1)} %maximum_bitcast_fusion, bf16[1,256,2048]{2,1,0:T(8,128)(2,1)} %bitcast.29, bf16[1,256,2048]{2,1,0:T(8,128)(2,1)} %bitcast.28), kind=kLoop, calls=%fused_computation.1 | loop fusion | flops 6291456 | bytes 8388608 | tf_op jit(solution)/shard_map/stack | solution.py:370
  134.7 3.1 %collective-permute-start.11 = (f32[48,768]{1,0:T(8,128)S(1)}, f32[48,768]{1,0:T(8,128)S(1)}, u32[]{:S(2)}, u32[]{:S(2)}) collective-permute-start(f32[48,768]{1,0:T(8,128)S(1)} %get-tuple-element.25.t0), channel_id=1, source_target_pairs={{0,24},{8,0},{16,8},{24,16},{1,25},{9,1},{17,9},{25,17},{2,26},{10... | collective-permute-start | bytes 442376 | tf_op jit(solution)/shard_map/ppermute | solution.py:431
  137.9 7.3 %collective-permute-done.13.t3 = f32[48,768]{1,0:T(8,128)S(1)} collective-permute-done((f32[48,768]{1,0:T(8,128)S(1)}, f32[48,768]{1,0:T(8,128)S(1)}, u32[]{:S(2)}, u32[]{:S(2)}) %collective-permute-start.13) | collective-permute-done | bytes 147488 | tf_op jit(solution)/shard_map/ppermute | solution.py:430
  145.8 7.3 %combine_key_blocks.1 = bf16[4,768,256]{2,1,0:T(8,128)(2,1)S(1)} custom-call(s32[2]{0:T(128)S(1)} %pad_add_fusion.1.place, bf16[16,768,256]{2,1,0:T(8,128)(2,1)S(1)} %get-tuple-element.24.outs, f32[48,768]{1,0:T(8,128)S(1)} %get-tuple-element.25.t0, f32[48,768]{1,0:T(8,128)S(1)} %collective-permute-done.11.t1, f32[48,768]{1,0:T(8,128)S(1)} %collective-permute-done.12.t2, ...), custom_call_target="tpu_custom_call" | custom-call | tf_op jit(solution)/shard_map/combine_key_blocks/pallas_call | solution.py:185
  160.1 11.1 %collective-permute-done.16 = bf16[384,256]{1,0:T(8,128)(2,1)S(1)} collective-permute-done((bf16[384,256]{1,0:T(8,128)(2,1)S(1)}, bf16[384,256]{1,0:T(8,128)(2,1)S(1)}, u32[]{:S(2)}, u32[]{:S(2)}) %collective-permute-start.16) | collective-permute-done | bytes 196640 | tf_op jit(solution)/shard_map/ppermute | solution.py:377
  174.2 3.3 %collective-permute-start.24 = (bf16[96,2048]{1,0:T(8,128)(2,1)S(1)}, bf16[96,2048]{1,0:T(8,128)(2,1)S(1)}, u32[]{:S(2)}, u32[]{:S(2)}) collective-permute-start(bf16[96,2048]{1,0:T(8,128)(2,1)S(1)} %copy-done.11), channel_id=1, source_target_pairs={{0,6},{2,0},{4,2},{6,4},{1,7},{3,1},{5,3},{7,5},{8,14},{10,8},{12,... | collective-permute-start | bytes 1179656 | tf_op jit(solution)/shard_map/ppermute | solution.py:427
  181.8 3.1 %collective-permute-done.24 = bf16[96,2048]{1,0:T(8,128)(2,1)S(1)} collective-permute-done((bf16[96,2048]{1,0:T(8,128)(2,1)S(1)}, bf16[96,2048]{1,0:T(8,128)(2,1)S(1)}, u32[]{:S(2)}, u32[]{:S(2)}) %collective-permute-start.24) | collective-permute-done | bytes 393248 | tf_op jit(solution)/shard_map/ppermute | solution.py:427
  184.9 3.8 %collective-permute-start.27 = (bf16[48,2048]{1,0:T(8,128)(2,1)S(1)}, bf16[48,2048]{1,0:T(8,128)(2,1)S(1)}, u32[]{:S(2)}, u32[]{:S(2)}) collective-permute-start(bf16[48,2048]{1,0:T(8,128)(2,1)S(1)} %slice.98), channel_id=1, source_target_pairs={{0,6},{2,0},{4,2},{6,4},{1,7},{3,1},{5,3},{7,5},{8,14},{10,8},{12,... | collective-permute-start | bytes 589832 | tf_op jit(solution)/shard_map/ppermute | solution.py:365
  188.7 3.2 %collective-permute-start.19 = (bf16[768,256]{1,0:T(8,128)(2,1)S(1)}, bf16[768,256]{1,0:T(8,128)(2,1)S(1)}, u32[]{:S(2)}, u32[]{:S(2)}) collective-permute-start(bf16[768,256]{1,0:T(8,128)(2,1)S(1)} %collective-permute-done.18), channel_id=1, source_target_pairs={{0,6},{2,0},{4,2},{6,4},{1,7},{3,1},{5,3},{7,5},{8,14},{10,8},{12,... | collective-permute-start | bytes 1179656 | tf_op jit(solution)/shard_map/ppermute | solution.py:353
  194.0 4.6 %collective-permute-done.20 = bf16[768,256]{1,0:T(8,128)(2,1)S(1)} collective-permute-done((bf16[768,256]{1,0:T(8,128)(2,1)S(1)}, bf16[768,256]{1,0:T(8,128)(2,1)S(1)}, u32[]{:S(2)}, u32[]{:S(2)}) %collective-permute-start.20) | collective-permute-done | bytes 393248 | tf_op jit(solution)/shard_map/ppermute | solution.py:352
  200.0 3.8 %collective-permute-start.22 = (bf16[384,256]{1,0:T(8,128)(2,1)S(1)}, bf16[384,256]{1,0:T(8,128)(2,1)S(1)}, u32[]{:S(2)}, u32[]{:S(2)}) collective-permute-start(bf16[384,256]{1,0:T(8,128)(2,1)S(1)} %slice.96), channel_id=1, source_target_pairs={{0,6},{2,0},{4,2},{6,4},{1,7},{3,1},{5,3},{7,5},{8,14},{10,8},{12,... | collective-permute-start | bytes 589832 | tf_op jit(solution)/shard_map/ppermute | solution.py:355
  211.1 23.8 %project_norm_mlp.1 = (f32[96,2048]{1,0:T(8,128)}, bf16[4,96,2048]{2,1,0:T(8,128)(2,1)}, bf16[4,96,2048]{2,1,0:T(8,128)(2,1)}) custom-call(s32[2]{0:T(128)} %pad_add_fusion.place, bf16[4,192,1024]{2,1,0:T(8,128)(2,1)} %bitcast.61, bf16[4,192,1024]{2,1,0:T(8,128)(2,1)} %bitcast.62, bf16[4,192,1024]{2,1,0:T(8,128)(2,1)} %bitcast.23.refs_2_.refs_3_, ...), custom_call_target="tpu_custom_call" | custom-call | tf_op jit(solution)/shard_map/project_norm_mlp/pallas_call | solution.py:300
  235.0 3.5 %collective-permute-done.32 = bf16[4,96,2048]{2,1,0:T(8,128)(2,1)S(1)} collective-permute-done((bf16[4,96,2048]{2,1,0:T(8,128)(2,1)}, bf16[4,96,2048]{2,1,0:T(8,128)(2,1)S(1)}, u32[]{:S(2)}, u32[]{:S(2)}) %collective-permute-start.32) | collective-permute-done | bytes 1572896 | tf_op jit(solution)/shard_map/ppermute | solution.py:347
  240.7 3.8 %collective-permute-start.34 = (bf16[96,2048]{1,0:T(8,128)(2,1)S(1)}, bf16[96,2048]{1,0:T(8,128)(2,1)S(1)}, u32[]{:S(2)}, u32[]{:S(2)}) collective-permute-start(bf16[96,2048]{1,0:T(8,128)(2,1)S(1)} %get-tuple-element.36), channel_id=1, source_target_pairs={{0,6},{2,0},{4,2},{6,4},{1,7},{3,1},{5,3},{7,5},{8,14},{10,8},{12,... | collective-permute-start | bytes 1179656 | tf_op jit(solution)/shard_map/ppermute | solution.py:376
  248.1 11.9 %collective-permute-done.35 = bf16[48,2048]{1,0:T(8,128)(2,1)S(1)} collective-permute-done((bf16[48,2048]{1,0:T(8,128)(2,1)S(1)}, bf16[48,2048]{1,0:T(8,128)(2,1)S(1)}, u32[]{:S(2)}, u32[]{:S(2)}) %collective-permute-start.35) | collective-permute-done | bytes 196640 | tf_op jit(solution)/shard_map/ppermute | solution.py:377
  260.0 3.4 %collective-permute-done.36 = bf16[48,2048]{1,0:T(8,128)(2,1)S(1)} collective-permute-done((bf16[48,2048]{1,0:T(8,128)(2,1)S(1)}, bf16[48,2048]{1,0:T(8,128)(2,1)S(1)}, u32[]{:S(2)}, u32[]{:S(2)}) %collective-permute-start.36) | collective-permute-done | bytes 196640 | tf_op jit(solution)/shard_map/ppermute | solution.py:378
  (148 shorter events, 70.8 us)
Async XLA Ops:
  6.5 204.5 %all-gather.2.cloned.1.call-start = ((), (), s32[]{:S(2)}) async-start(), calls=%async_computation | async-start | bytes 9469952 | tf_op jit(solution)/shard_map/all_gather | solution.py:414
  11.1 25.0 %collective-permute-start.1 = (bf16[768,256]{1,0:T(8,128)(2,1)S(1)}, bf16[768,256]{1,0:T(8,128)(2,1)S(1)}, u32[]{:S(2)}, u32[]{:S(2)}) collective-permute-start(bf16[768,256]{1,0:T(8,128)(2,1)S(1)} %collective-permute-done), channel_id=1, source_target_pairs={{0,24},{8,0},{16,8},{24,16},{1,25},{9,1},{17,9},{25,17},{2,26},{10... | collective-permute-start | bytes 1179656 | tf_op jit(solution)/shard_map/ppermute | solution.py:411
  36.1 24.1 %collective-permute-start.6 = (bf16[784,512]{1,0:T(8,128)(2,1)S(1)}, bf16[784,512]{1,0:T(8,128)(2,1)S(1)}, u32[]{:S(2)}, u32[]{:S(2)}) collective-permute-start(bf16[784,512]{1,0:T(8,128)(2,1)S(1)} %fusion.1), channel_id=1, source_target_pairs={{0,32},{32,64},{64,96},{96,0},{1,33},{33,65},{65,97},{97,1},{2,34}... | collective-permute-start | bytes 2408456 | tf_op jit(solution)/shard_map/ppermute | solution.py:407
  36.8 30.3 %collective-permute-start.5 = (bf16[784,512]{1,0:T(8,128)(2,1)S(1)}, bf16[784,512]{1,0:T(8,128)(2,1)S(1)}, u32[]{:S(2)}, u32[]{:S(2)}) collective-permute-start(bf16[784,512]{1,0:T(8,128)(2,1)S(1)} %fusion.1), channel_id=1, source_target_pairs={{0,96},{32,0},{64,32},{96,64},{1,97},{33,1},{65,33},{97,65},{2,98}... | collective-permute-start | bytes 2408456 | tf_op jit(solution)/shard_map/ppermute | solution.py:408
  39.4 11.0 %collective-permute-start.2 = (bf16[768,256]{1,0:T(8,128)(2,1)}, bf16[768,256]{1,0:T(8,128)(2,1)S(1)}, u32[]{:S(2)}, u32[]{:S(2)}) collective-permute-start(bf16[768,256]{1,0:T(8,128)(2,1)} %copy-done.12), channel_id=1, source_target_pairs={{0,8},{8,16},{16,24},{24,0},{1,9},{9,17},{17,25},{25,1},{2,10},{10... | collective-permute-start | bytes 1179656 | tf_op jit(solution)/shard_map/ppermute | solution.py:410
  44.2 73.0 %collective-permute-start.10 = (bf16[256,2048]{1,0:T(8,128)(2,1)}, bf16[256,2048]{1,0:T(8,128)(2,1)}, u32[]{:S(2)}, u32[]{:S(2)}) collective-permute-start(bf16[256,2048]{1,0:T(8,128)(2,1)} %constant_dynamic-update-slice_fusion), channel_id=1, source_target_pairs={{0,6},{2,0},{4,2},{6,4},{1,7},{3,1},{5,3},{7,5},{8,14},{10,8},{12,... | collective-permute-start | bytes 3145736 | tf_op jit(solution)/shard_map/ppermute | solution.py:419
  47.2 70.0 %collective-permute-start.9 = (bf16[256,2048]{1,0:T(8,128)(2,1)}, bf16[256,2048]{1,0:T(8,128)(2,1)}, u32[]{:S(2)}, u32[]{:S(2)}) collective-permute-start(bf16[256,2048]{1,0:T(8,128)(2,1)} %constant_dynamic-update-slice_fusion), channel_id=1, source_target_pairs={{0,2},{2,4},{4,6},{6,0},{1,3},{3,5},{5,7},{7,1},{8,10},{10,12},{12... | collective-permute-start | bytes 3145736 | tf_op jit(solution)/shard_map/ppermute | solution.py:418
  51.2 16.7 %collective-permute-start.3 = (bf16[384,256]{1,0:T(8,128)(2,1)}, bf16[384,256]{1,0:T(8,128)(2,1)}, u32[]{:S(2)}, u32[]{:S(2)}) collective-permute-start(bf16[384,256]{1,0:T(8,128)(2,1)} %slice.86), channel_id=1, source_target_pairs={{0,8},{8,16},{16,24},{24,0},{1,9},{9,17},{17,25},{25,1},{2,10},{10... | collective-permute-start | bytes 589832 | tf_op jit(solution)/shard_map/ppermute | solution.py:364
  60.2 11.0 %collective-permute-start.4 = (bf16[384,256]{1,0:T(8,128)(2,1)S(1)}, bf16[384,256]{1,0:T(8,128)(2,1)}, u32[]{:S(2)}, u32[]{:S(2)}) collective-permute-start(bf16[384,256]{1,0:T(8,128)(2,1)S(1)} %slice.64), channel_id=1, source_target_pairs={{0,24},{8,0},{16,8},{24,16},{1,25},{9,1},{17,9},{25,17},{2,26},{10... | collective-permute-start | bytes 589832 | tf_op jit(solution)/shard_map/ppermute | solution.py:365
  67.9 10.7 %collective-permute-start.8 = (bf16[392,512]{1,0:T(8,128)(2,1)}, bf16[392,512]{1,0:T(8,128)(2,1)}, u32[]{:S(2)}, u32[]{:S(2)}) collective-permute-start(bf16[392,512]{1,0:T(8,128)(2,1)} %slice.88), channel_id=1, source_target_pairs={{0,96},{32,0},{64,32},{96,64},{1,97},{33,1},{65,33},{97,65},{2,98}... | collective-permute-start | bytes 1204232 | tf_op jit(solution)/shard_map/ppermute | solution.py:365
  119.3 11.4 %collective-permute-start.29 = (bf16[128,2048]{1,0:T(8,128)(2,1)S(1)}, bf16[128,2048]{1,0:T(8,128)(2,1)S(1)}, u32[]{:S(2)}, u32[]{:S(2)}) collective-permute-start(bf16[128,2048]{1,0:T(8,128)(2,1)S(1)} %slice.77), channel_id=1, source_target_pairs={{0,2},{2,4},{4,6},{6,0},{1,3},{3,5},{5,7},{7,1},{8,10},{10,12},{12... | collective-permute-start | bytes 1572872 | tf_op jit(solution)/shard_map/ppermute | solution.py:364
  134.6 76.5 %collective-permute-start.31 = (bf16[1024,2048]{1,0:T(8,128)(2,1)}, bf16[1024,2048]{1,0:T(8,128)(2,1)}, u32[]{:S(2)}, u32[]{:S(2)}) collective-permute-start(bf16[1024,2048]{1,0:T(8,128)(2,1)} %bitcast.32.refs_7_), channel_id=1, source_target_pairs={{0,1},{1,0},{2,3},{3,2},{4,5},{5,4},{6,7},{7,6},{8,9},{9,8},{10,11... | collective-permute-start | bytes 12582920 | tf_op jit(solution)/shard_map/ppermute | solution.py:347
  134.7 11.2 %collective-permute-start.11 = (f32[48,768]{1,0:T(8,128)S(1)}, f32[48,768]{1,0:T(8,128)S(1)}, u32[]{:S(2)}, u32[]{:S(2)}) collective-permute-start(f32[48,768]{1,0:T(8,128)S(1)} %get-tuple-element.25.t0), channel_id=1, source_target_pairs={{0,24},{8,0},{16,8},{24,16},{1,25},{9,1},{17,9},{25,17},{2,26},{10... | collective-permute-start | bytes 442376 | tf_op jit(solution)/shard_map/ppermute | solution.py:431
  153.2 24.3 %collective-permute-start.14 = (bf16[768,256]{1,0:T(8,128)(2,1)S(1)}, bf16[768,256]{1,0:T(8,128)(2,1)S(1)}, u32[]{:S(2)}, u32[]{:S(2)}) collective-permute-start(bf16[768,256]{1,0:T(8,128)(2,1)S(1)} %get-tuple-element.39), channel_id=1, source_target_pairs={{0,8},{8,16},{16,24},{24,0},{1,9},{9,17},{17,25},{25,1},{2,10},{10... | collective-permute-start | bytes 1179656 | tf_op jit(solution)/shard_map/ppermute | solution.py:375
  153.5 24.0 %collective-permute-start.15 = (bf16[768,256]{1,0:T(8,128)(2,1)S(1)}, bf16[768,256]{1,0:T(8,128)(2,1)S(1)}, u32[]{:S(2)}, u32[]{:S(2)}) collective-permute-start(bf16[768,256]{1,0:T(8,128)(2,1)S(1)} %get-tuple-element.40), channel_id=1, source_target_pairs={{0,24},{8,0},{16,8},{24,16},{1,25},{9,1},{17,9},{25,17},{2,26},{10... | collective-permute-start | bytes 1179656 | tf_op jit(solution)/shard_map/ppermute | solution.py:376
  156.5 14.7 %collective-permute-start.16 = (bf16[384,256]{1,0:T(8,128)(2,1)S(1)}, bf16[384,256]{1,0:T(8,128)(2,1)S(1)}, u32[]{:S(2)}, u32[]{:S(2)}) collective-permute-start(bf16[384,256]{1,0:T(8,128)(2,1)S(1)} %get-tuple-element.37), channel_id=1, source_target_pairs={{0,16},{8,24},{16,0},{24,8},{1,17},{9,25},{17,1},{25,9},{2,18},{10... | collective-permute-start | bytes 589832 | tf_op jit(solution)/shard_map/ppermute | solution.py:377
  157.2 17.0 %collective-permute-start.17 = (bf16[384,256]{1,0:T(8,128)(2,1)S(1)}, bf16[384,256]{1,0:T(8,128)(2,1)S(1)}, u32[]{:S(2)}, u32[]{:S(2)}) collective-permute-start(bf16[384,256]{1,0:T(8,128)(2,1)S(1)} %get-tuple-element.38), channel_id=1, source_target_pairs={{0,16},{8,24},{16,0},{24,8},{1,17},{9,25},{17,1},{25,9},{2,18},{10... | collective-permute-start | bytes 589832 | tf_op jit(solution)/shard_map/ppermute | solution.py:378
  174.2 10.7 %collective-permute-start.24 = (bf16[96,2048]{1,0:T(8,128)(2,1)S(1)}, bf16[96,2048]{1,0:T(8,128)(2,1)S(1)}, u32[]{:S(2)}, u32[]{:S(2)}) collective-permute-start(bf16[96,2048]{1,0:T(8,128)(2,1)S(1)} %copy-done.11), channel_id=1, source_target_pairs={{0,6},{2,0},{4,2},{6,4},{1,7},{3,1},{5,3},{7,5},{8,14},{10,8},{12,... | collective-permute-start | bytes 1179656 | tf_op jit(solution)/shard_map/ppermute | solution.py:427
  177.7 11.0 %collective-permute-start.18 = (bf16[768,256]{1,0:T(8,128)(2,1)S(1)}, bf16[768,256]{1,0:T(8,128)(2,1)S(1)}, u32[]{:S(2)}, u32[]{:S(2)}) collective-permute-start(bf16[768,256]{1,0:T(8,128)(2,1)S(1)} %fusion.7), channel_id=1, source_target_pairs={{0,0},{8,8},{48,16},{56,24},{64,32},{72,40},{112,48},{120,56},{96,... | collective-permute-start | bytes 1179656 | tf_op jit(solution)/shard_map/ppermute | solution.py:440
  188.7 11.3 %collective-permute-start.19 = (bf16[768,256]{1,0:T(8,128)(2,1)S(1)}, bf16[768,256]{1,0:T(8,128)(2,1)S(1)}, u32[]{:S(2)}, u32[]{:S(2)}) collective-permute-start(bf16[768,256]{1,0:T(8,128)(2,1)S(1)} %collective-permute-done.18), channel_id=1, source_target_pairs={{0,6},{2,0},{4,2},{6,4},{1,7},{3,1},{5,3},{7,5},{8,14},{10,8},{12,... | collective-permute-start | bytes 1179656 | tf_op jit(solution)/shard_map/ppermute | solution.py:353
  240.6 22.8 %collective-permute-start.33 = (bf16[96,2048]{1,0:T(8,128)(2,1)S(1)}, bf16[96,2048]{1,0:T(8,128)(2,1)S(1)}, u32[]{:S(2)}, u32[]{:S(2)}) collective-permute-start(bf16[96,2048]{1,0:T(8,128)(2,1)S(1)} %get-tuple-element.35), channel_id=1, source_target_pairs={{0,2},{2,4},{4,6},{6,0},{1,3},{3,5},{5,7},{7,1},{8,10},{10,12},{12... | collective-permute-start | bytes 1179656 | tf_op jit(solution)/shard_map/ppermute | solution.py:375
  240.7 22.7 %collective-permute-start.34 = (bf16[96,2048]{1,0:T(8,128)(2,1)S(1)}, bf16[96,2048]{1,0:T(8,128)(2,1)S(1)}, u32[]{:S(2)}, u32[]{:S(2)}) collective-permute-start(bf16[96,2048]{1,0:T(8,128)(2,1)S(1)} %get-tuple-element.36), channel_id=1, source_target_pairs={{0,6},{2,0},{4,2},{6,4},{1,7},{3,1},{5,3},{7,5},{8,14},{10,8},{12,... | collective-permute-start | bytes 1179656 | tf_op jit(solution)/shard_map/ppermute | solution.py:376
  244.5 15.5 %collective-permute-start.35 = (bf16[48,2048]{1,0:T(8,128)(2,1)S(1)}, bf16[48,2048]{1,0:T(8,128)(2,1)S(1)}, u32[]{:S(2)}, u32[]{:S(2)}) collective-permute-start(bf16[48,2048]{1,0:T(8,128)(2,1)S(1)} %get-tuple-element.33), channel_id=1, source_target_pairs={{0,4},{2,6},{4,0},{6,2},{1,5},{3,7},{5,1},{7,3},{8,12},{10,14},{12... | collective-permute-start | bytes 589832 | tf_op jit(solution)/shard_map/ppermute | solution.py:377
  246.0 17.4 %collective-permute-start.36 = (bf16[48,2048]{1,0:T(8,128)(2,1)S(1)}, bf16[48,2048]{1,0:T(8,128)(2,1)S(1)}, u32[]{:S(2)}, u32[]{:S(2)}) collective-permute-start(bf16[48,2048]{1,0:T(8,128)(2,1)S(1)} %get-tuple-element.34), channel_id=1, source_target_pairs={{0,4},{2,6},{4,0},{6,2},{1,5},{3,7},{5,1},{7,3},{8,12},{10,14},{12... | collective-permute-start | bytes 589832 | tf_op jit(solution)/shard_map/ppermute | solution.py:378
  (33 other events, 327.2 us)
Sparse Core Ops, SparseCore 0:
  36.2 79.2 all-gather.1
